TPU v7x, 32 devices: a whole 2x2x4 slice. The times are simulated.
32 devices in a mesh: fs: 4 (over z), tp: 8 (over y, x, core).
Axes of the slice: x: 2, y: 2, z: 4, core: 2. Of those that a mesh axis runs over, the one named last changes fastest.
Arguments:
- inputs: bfloat16 [1024, 2016], P('fs'), may hold values from -6 to 6
- pre_act: bfloat16 [1024, 4032], P('fs', 'tp'), may hold values from -6 to 6
- cotangent: bfloat16 [1024, 2016], P('fs'), may hold values from -6 to 6
- w_up: bfloat16 [2016, 4032], P('fs', 'tp'), may hold values from -0.125 to 0.125
- w_down: bfloat16 [4032, 2016], P('tp', 'fs'), may hold values from -0.09375 to 0.09375
Outputs:
- grad_input: bfloat16 [1024, 2016], P('fs')
- grad_up: float32 [2016, 4032], P('fs', 'tp')
- grad_down: float32 [4032, 2016], P('tp', 'fs')
All inputs are finite; a program needn't handle non-finite values.
Results may differ from a plain program's by a relative error of at most 0.017.
Values may be sent and summed in bfloat16 or wider, within the bound.
No kernel may reach another device: no remote copies, remote signals or barrier semaphores. Data moves between devices by JAX's collectives and lax.ppermute only.
A program may use at most 64 MiB of HBM per device.

v0:
```python
import jax
import jax.numpy as jnp
from jax import lax
from jax.sharding import PartitionSpec as P


def on_device(inputs, pre_act, cotangent, w_up, w_down):
    positive = jnp.maximum(pre_act.astype(jnp.float32), 0.0)
    hidden = (positive * positive).astype(jnp.bfloat16)
    columns = cotangent
    hidden_grad = lax.dot_general(
        columns,
        lax.all_gather(w_down, "fs", axis=1, tiled=True),
        (((1,), (1,)), ((), ())),
        preferred_element_type=jnp.float32,
    )
    pre_grad = (2.0 * positive * hidden_grad).astype(jnp.bfloat16)
    columns = inputs
    grad_up = lax.psum_scatter(
        lax.dot_general(
            columns, pre_grad, (((0,), (0,)), ((), ())), preferred_element_type=jnp.float32
        ).astype(jnp.bfloat16),
        "fs",
        scatter_dimension=0,
        tiled=True,
    ).astype(jnp.float32)
    columns = cotangent
    grad_down = (
        lax.psum_scatter(
            lax.dot_general(
                columns, hidden, (((0,), (0,)), ((), ())), preferred_element_type=jnp.float32
            ).astype(jnp.bfloat16),
            "fs",
            scatter_dimension=0,
            tiled=True,
        )
        .astype(jnp.float32)
        .T
    )
    partial_sum = lax.dot_general(
        pre_grad,
        lax.all_gather(w_up, "fs", axis=0, tiled=True),
        (((1,), (1,)), ((), ())),
        preferred_element_type=jnp.float32,
    ).astype(jnp.bfloat16)
    shares = (
        lax.psum_scatter(partial_sum, "tp", scatter_dimension=0, tiled=True)
        .astype(jnp.float32)
        .astype(jnp.bfloat16)
    )
    grad_input = lax.all_gather(shares, "tp", axis=0, tiled=True)
    return (grad_input, grad_up, grad_down)


def solution(mesh):
    in_specs = (P("fs", None), P("fs", "tp"), P("fs", None), P("fs", "tp"), P("tp", "fs"))
    out_specs = (P("fs", None), P("fs", "tp"), P("tp", "fs"))
    return jax.shard_map(
        on_device, mesh=mesh, in_specs=in_specs, out_specs=out_specs, check_vma=False
    )
```

profile of v0, /device:TPU:0, one launch (start us, length us, event | category | flops | bytes accessed | tf_op | source)
XLA Modules:
  0.0 240.3 jit_solution(424361379312722915)
XLA Ops:
  7.2 0.0 all-gather.3.cloned.1.call-start
  7.2 2.1 copy.10
  9.4 0.0 all-gather.5.cloned.1.call-start
  9.4 0.7 all-gather.5.cloned.1.call-update
  10.1 0.0 reduce-scatter.12.cloned.1.call-start
  10.2 0.7 fusion.1
  11.0 2.4 %copy.15 = bf16[2016,504]{1,0:T(8,128)(2,1)} copy(bf16[2016,504]{0,1:T(8,128)(2,1)S(1)} %fusion.1) | data formatting | bytes 4064256
  13.4 0.0 reduce-scatter.8.cloned.1.call-start
  13.5 44.5 %all-gather.3.cloned.1.call-done = bf16[504,2016]{0,1:T(8,128)(2,1)} async-done(((bf16[504,504]{0,1:T(8,128)(2,1)}), bf16[504,2016]{0,1:T(8,128)(2,1)}) %all-gather.3.cloned.1.call-update) | async-done | bytes 2032144 | tf_op jit(solution)/shard_map/all_gather | solution.py:13
  58.0 2.5 %fusion.2 = bf16[256,504]{0,1:T(8,128)(2,1)S(1)} fusion(bf16[256,2016]{0,1:T(8,128)(2,1)S(1)} %copy-done, bf16[504,2016]{0,1:T(8,128)(2,1)} %all-gather.3.cloned.1.call-done, bf16[256,504]{0,1:T(8,128)(2,1)S(1)} %copy-done.1), kind=kOutput, calls=%fused_computation.6 | convolution fusion | flops 520869888 | bytes 3580416 | tf_op jit(solution)/shard_map/dot_general | solution.py:11
  60.5 43.0 %all-gather.5.cloned.1.call-done = bf16[2016,504]{1,0:T(8,128)(2,1)} async-done(((bf16[504,504]{1,0:T(8,128)(2,1)}), bf16[2016,504]{1,0:T(8,128)(2,1)}) %all-gather.5.cloned.1.call-update) | async-done | bytes 2032144 | tf_op jit(solution)/shard_map/all_gather | solution.py:42
  103.5 3.3 %convolution_convert_fusion.2 = bf16[256,2016]{1,0:T(8,128)(2,1)} fusion(bf16[256,504]{0,1:T(8,128)(2,1)S(1)} %fusion.2, bf16[2016,504]{1,0:T(8,128)(2,1)} %all-gather.5.cloned.1.call-done), kind=kOutput, calls=%fused_computation.4 | convolution fusion | flops 520740864 | bytes 3322368 | tf_op jit(solution)/shard_map/dot_general | solution.py:40
  106.9 0.0 reduce-scatter.10.cloned.1.call-start
  106.9 2.0 fusion
  108.9 2.4 %copy.13 = bf16[2016,504]{1,0:T(8,128)(2,1)} copy(bf16[2016,504]{0,1:T(8,128)(2,1)S(1)} %fusion) | data formatting | bytes 4064256
  111.4 36.5 %reduce-scatter.12.cloned.1.call-done = bf16[504,504]{1,0:T(8,128)(2,1)} async-done(((bf16[2016,504]{1,0:T(8,128)(2,1)}), bf16[504,504]{1,0:T(8,128)(2,1)}) %reduce-scatter.12.cloned.1.call-update) | async-done | bytes 508048
  147.9 1.2 copy.16
  149.1 1.1 convert_bitcast_fusion
  150.2 35.9 %reduce-scatter.8.cloned.1.call-done = bf16[32,2016]{1,0:T(8,128)(2,1)} async-done(((bf16[256,2016]{1,0:T(8,128)(2,1)}), bf16[32,2016]{1,0:T(8,128)(2,1)}) %reduce-scatter.8.cloned.1.call-update) | async-done | bytes 129040 | tf_op jit(solution)/shard_map/reduce_scatter | solution.py:47
  186.1 10.9 %all_gather.11 = bf16[256,2016]{1,0:T(8,128)(2,1)S(1)} all-gather(bf16[32,2016]{1,0:T(8,128)(2,1)} %reduce-scatter.8.cloned.1.call-done), channel_id=1, replica_groups=mesh['fs'=4,'tp'=8] {'tp'}, dimensions={0}, use_global_device_ids=true | all-gather | bytes 1161216 | tf_op jit(solution)/shard_map/all_gather | solution.py:51
  197.0 1.3 copy.11
  198.3 33.1 %reduce-scatter.10.cloned.1.call-done = bf16[504,504]{1,0:T(8,128)(2,1)} async-done(((bf16[2016,504]{1,0:T(8,128)(2,1)}), bf16[504,504]{1,0:T(8,128)(2,1)}) %reduce-scatter.10.cloned.1.call-update) | async-done | bytes 508048
  231.4 1.2 copy.14
  232.6 1.2 copy.12
  (8 shorter events, 0.1 us)
Async XLA Ops:
  7.2 3.0 %copy-start = (bf16[256,2016]{0,1:T(8,128)(2,1)S(1)}, bf16[256,2016]{0,1:T(8,128)(2,1)}, u32[]{:S(2)}) copy-start(bf16[256,2016]{0,1:T(8,128)(2,1)} %param.7) | copy-start | bytes 3096580
  7.2 3.0 %copy-start.1 = (bf16[256,504]{0,1:T(8,128)(2,1)S(1)}, bf16[256,504]{0,1:T(8,128)(2,1)}, u32[]{:S(2)}) copy-start(bf16[256,504]{0,1:T(8,128)(2,1)} %param.6) | copy-start | bytes 774148
  7.2 50.8 %all-gather.3.cloned.1.call-start = ((), (), s32[]{:S(2)}) async-start(), calls=%async_computation.3 | async-start | bytes 2580480 | tf_op jit(solution)/shard_map/all_gather | solution.py:13
  9.4 94.2 %all-gather.5.cloned.1.call-start = ((), (), s32[]{:S(2)}) async-start(), calls=%async_computation.4 | async-start | bytes 2580480 | tf_op jit(solution)/shard_map/all_gather | solution.py:42
  10.1 137.7 %reduce-scatter.12.cloned.1.call-start = ((), (), s32[]{:S(2)}) async-start(), calls=%async_computation.7 | async-start | bytes 2580480
  13.4 172.6 %reduce-scatter.8.cloned.1.call-start = ((), (), s32[]{:S(2)}) async-start(), calls=%async_computation.5 | async-start | bytes 1179648 | tf_op jit(solution)/shard_map/reduce_scatter | solution.py:47
  106.9 124.5 %reduce-scatter.10.cloned.1.call-start = ((), (), s32[]{:S(2)}) async-start(), calls=%async_computation.6 | async-start | bytes 2580480
Sparse Core Ops, SparseCore 0:
  10.1 47.8 all-gather.2
  59.6 43.9 all-gather.4
  105.9 41.9 reduce-scatter.11
  150.9 35.1 reduce-scatter.7
  188.2 43.0 reduce-scatter.9
where the time goes:
time: 241 us; the launch traced here: 240 us
  waiting for transfers between devices  194 us (80%)
  between operations  13.8 us (6%)
  local copies, waits for them, and re-layouts  12 us (5%)
  blocking collectives  10.9 us (5%)
  matrix products  8.52 us (4%)
    unnamed x7, waiting for transfers between devices  70.4 us
    all_gather x1, waiting for transfers between devices, on_device(): lax.all_gather(w_down, 'fs', axis=1, tiled=True)  44.5 us
    all_gather x1, waiting for transfers between devices, on_device(): lax.all_gather(w_up, 'fs', axis=0, tiled=True)  43 us
    reduce_scatter x1, waiting for transfers between devices, on_device(): lax.psum_scatter(partial_sum, 'tp', scatter_dimension=0, tiled=True)  35.9 us
    unnamed x11, local copies, waits for them, and re-layouts  12 us
    all_gather x1, blocking collectives, on_device(): grad_input = lax.all_gather(shares, 'tp', axis=0, tiled=True)  10.9 us
  transfers between devices with their start and end apart: 5, of which 5 were waited for; matrix products, arithmetic and copies ran while one was open for 7% of the time, Pallas kernels for 0%

commit v1 on v0

v1 whole, which is shorter than its diff:
```python
import jax
import jax.numpy as jnp
from jax import lax
from jax.sharding import PartitionSpec as P

F32, BF16 = jnp.float32, jnp.bfloat16


def dot(a, b, ca, cb):
    return lax.dot_general(a, b, (((ca,), (cb,)), ((), ())), preferred_element_type=F32)


def body(inputs, pre_act, cotangent, w_up, w_down, n_fs, n_tp):
    groups = n_fs // 2
    tokens, width = inputs.shape
    block = width // n_fs
    share = tokens // n_tp
    me = lax.axis_index("fs")
    group, side = me // 2, me % 2
    lane = lax.axis_index("tp")

    sibling = [(p, p ^ 1) for p in range(n_fs)]

    def shift(x, k):
        return lax.ppermute(x, "fs", [(p, (p + 2 * k) % n_fs) for p in range(n_fs)])

    def columns(x, row, rows, k):
        base = 2 * ((group + k) % groups)
        own = lax.dynamic_slice(x, (row, (base + side) * block), (rows, block))
        other = lax.dynamic_slice(x, (row, (base + 1 - side) * block), (rows, block))
        return jnp.concatenate([own, other], axis=1)

    cot_shares = [shift(columns(cotangent, lane * share, share, k), k) for k in range(1, groups)]
    w_down_g = jnp.concatenate([w_down, lax.ppermute(w_down, "fs", sibling)], axis=1)
    cot = [columns(cotangent, 0, tokens, 0)]
    cot += [lax.all_gather(s, "tp", axis=0, tiled=True) for s in cot_shares]

    partial = [dot(c, w_down_g, 1, 1) for c in cot]
    hidden_grad = partial[0]
    for k in range(1, groups):
        hidden_grad = hidden_grad + shift(partial[k].astype(BF16), -k).astype(F32)
    positive = jnp.maximum(pre_act.astype(F32), 0.0)
    pre_grad = [(2.0 * positive * hidden_grad).astype(BF16)]
    pre_grad += [shift(pre_grad[0], k) for k in range(1, groups)]

    acts = [pre_act] + [shift(pre_act, k) for k in range(1, groups)]
    in_shares = [shift(columns(inputs, lane * share, share, k), k) for k in range(1, groups)]
    ins = [columns(inputs, 0, tokens, 0)]
    ins += [lax.all_gather(s, "tp", axis=0, tiled=True) for s in in_shares]
    w_up_g = jnp.concatenate([w_up, lax.ppermute(w_up, "fs", sibling)], axis=0)

    pieces = []
    for k in range(groups):
        terms = dot(pre_grad[k], w_up_g, 1, 1).astype(BF16)
        terms = lax.all_to_all(terms.reshape(n_tp, share, 2 * block), "tp", 0, 0)
        total = jnp.sum(terms.astype(F32), axis=0).astype(BF16)
        pieces.append(total if k == 0 else shift(total, -k))
    pairs = [p[:, :block] for p in pieces], [p[:, block:] for p in pieces]
    ordered = []
    for h in range(groups):
        at = (h - group) % groups
        own, other = pairs[0][0], pairs[1][0]
        for k in range(1, groups):
            own = jnp.where(at == k, pairs[0][k], own)
            other = jnp.where(at == k, pairs[1][k], other)
        ordered += [jnp.where(side == 0, own, other), jnp.where(side == 0, other, own)]
    grad_input = lax.all_gather(jnp.concatenate(ordered, axis=1), "tp", axis=0, tiled=True)

    hidden = []
    for a in acts:
        pos = jnp.maximum(a.astype(F32), 0.0)
        hidden.append((pos * pos).astype(BF16))

    def summed(terms):
        total = terms[0]
        for t in terms[1:]:
            total = total + t
        return total

    down_own = summed([dot(h, c[:, :block], 0, 0) for h, c in zip(hidden, cot)])
    down_other = summed([dot(h, c[:, block:], 0, 0) for h, c in zip(hidden, cot)])
    grad_down = down_own + lax.ppermute(down_other.astype(BF16), "fs", sibling).astype(F32)
    up_own = summed([dot(x[:, :block], p, 0, 0) for x, p in zip(ins, pre_grad)])
    up_other = summed([dot(x[:, block:], p, 0, 0) for x, p in zip(ins, pre_grad)])
    grad_up = up_own + lax.ppermute(up_other.astype(BF16), "fs", sibling).astype(F32)
    return grad_input, grad_up, grad_down


def solution(mesh):
    n_fs, n_tp = mesh.shape["fs"], mesh.shape["tp"]
    in_specs = (P("fs", None), P("fs", "tp"), P("fs", None), P("fs", "tp"), P("tp", "fs"))
    out_specs = (P("fs", None), P("fs", "tp"), P("tp", "fs"))

    def on_device(*args):
        return body(*args, n_fs, n_tp)

    return jax.shard_map(
        on_device, mesh=mesh, in_specs=in_specs, out_specs=out_specs, check_vma=False
    )
```

time: 241 us -> 110 us (0.46)
  waiting for transfers between devices: 194 us -> 26.2 us
  starting transfers between devices: 0.2 us -> 21 us
  blocking collectives: 10.9 us -> 31.3 us
  between operations: 13.8 us -> 0.91 us
  matrix products: 8.52 us -> 19.1 us
  local copies, waits for them, and re-layouts: 12 us -> 8.61 us
    all_gather x2 -> x0, waiting for transfers between devices: 87.6 us -> none  [the longest x1 44.5 us: on_device(): lax.all_gather(w_down, 'fs', axis=1, tiled=True)]
    unnamed x7 -> x0, waiting for transfers between devices: 70.4 us -> none
    reduce_scatter x1 -> x0, waiting for transfers between devices: 35.9 us -> none  [on_device(): lax.psum_scatter(partial_sum, 'tp', scatter_dimension=0, tiled=True)]
    all_gather x1 -> x3, blocking collectives: 10.9 us -> 31.3 us  [the longest x1 10.9 us: body(): ins += [lax.all_gather(s, 'tp', axis=0, tiled=True) for s in in_shares]]
    ppermute x0 -> x10, waiting for transfers between devices: none -> 19.5 us  [the longest x6 19.5 us: shift(): return lax.ppermute(x, 'fs', [(p, (p + 2 * k) % n_fs) for p in range(n_fs)])]
    ppermute x0 -> x10, starting transfers between devices: none -> 13.3 us  [the longest x6 9.36 us: shift(): return lax.ppermute(x, 'fs', [(p, (p + 2 * k) % n_fs) for p in range(n_fs)])]
    dot_general x4 -> x12, matrix products: 8.52 us -> 19.1 us  [dot(): lax.dot_general(a, b, (((ca,), (cb,)), ((), ())), preferred_element_type=...]
    unnamed x11 -> x20, local copies, waits for them, and re-layouts: 12 us -> 2.92 us
  transfers between devices with their start and end apart: 5 -> 12, of which waited for: 5 -> 4; matrix products, arithmetic and copies ran while one was open for 7% -> 24% of each run, Pallas kernels for 0% -> 0%
where the time goes in v1:
time: 110 us; the launch traced here: 109 us
  blocking collectives  31.3 us (28%)
  waiting for transfers between devices  26.2 us (24%)
  starting transfers between devices  21 us (19%)
  matrix products  19.1 us (17%)
  local copies, waits for them, and re-layouts  8.61 us (8%)
  other arithmetic  2.11 us (2%)
    ppermute x6, waiting for transfers between devices, shift(): return lax.ppermute(x, 'fs', [(p, (p + 2 * k) % n_fs) for p in range(n_fs)])  19.5 us
    dot_general x12, matrix products, dot(): lax.dot_general(a, b, (((ca,), (cb,)), ((), ())), preferred_element_type=...  19.1 us
    all_gather x1, blocking collectives, body(): ins += [lax.all_gather(s, 'tp', axis=0, tiled=True) for s in in_shares]  10.9 us
    all_gather x1, blocking collectives, body(): lax.all_gather(jnp.concatenate(ordered, axis=1), 'tp', axis=0, tiled=True)  10.7 us
    all_gather x1, blocking collectives, body(): cot += [lax.all_gather(s, 'tp', axis=0, tiled=True) for s in cot_shares]  9.73 us
    ppermute x6, starting transfers between devices, shift(): return lax.ppermute(x, 'fs', [(p, (p + 2 * k) % n_fs) for p in range(n_fs)])  9.36 us
    all_to_all x2, starting transfers between devices, body(): terms = lax.all_to_all(terms.reshape(n_tp, share, 2 * block), 'tp', 0, 0)  7.65 us
    all_to_all x2, waiting for transfers between devices, body(): terms = lax.all_to_all(terms.reshape(n_tp, share, 2 * block), 'tp', 0, 0)  6.7 us
  transfers between devices with their start and end apart: 12, of which 4 were waited for; matrix products, arithmetic and copies ran while one was open for 24% of the time, Pallas kernels for 0%

profile of v1, /device:TPU:0, one launch (start us, length us, event | category | flops | bytes accessed | tf_op | source)
XLA Modules:
  0.0 109.3 jit_solution(16990785984074586437)
XLA Ops:
  0.7 1.4 %fusion.27 = (bf16[32,504]{0,1:T(8,128)(2,1)S(1)}, bf16[32,504]{0,1:T(8,128)(2,1)S(1)}, bf16[32,504]{0,1:T(8,128)(2,1)S(1)}, bf16[32,504]{0,1:T(8,128)(2,1)S(1)}) fusion(bf16[256,2016]{0,1:T(8,128)(2,1)} %param.5, s32[]{:T(128)S(6)} %select_n.101, s32[]{:T(128)S(6)} %select_n.103, s32[]{:T(128)S(6)} %select_n.104, bf16[256,2016]{0,1:T(8,128)(2,1)} %param.7), kind=kLoop, calls=%fused_computation.53 | loop fusion | bytes 258060 | tf_op jit(solution)/shard_map/dynamic_slice | solution.py:29
  2.5 4.1 %collective-permute-start.6 = (bf16[32,1008]{1,0:T(8,128)(2,1)S(1)}, bf16[32,1008]{1,0:T(8,128)(2,1)S(1)}, u32[]{:S(2)}, u32[]{:S(2)}) collective-permute-start(bf16[32,1008]{1,0:T(8,128)(2,1)S(1)} %pad_maximum_fusion.4), channel_id=1, source_target_pairs={{0,16},{8,24},{16,0},{24,8},{1,17},{9,25},{17,1},{25,9},{2,18},{10... | collective-permute-start | bytes 193544 | tf_op jit(solution)/shard_map/ppermute | solution.py:25
  7.6 1.9 %collective-permute-start = (bf16[504,504]{1,0:T(8,128)(2,1)}, bf16[504,504]{1,0:T(8,128)(2,1)}, u32[]{:S(2)}, u32[]{:S(2)}) collective-permute-start(bf16[504,504]{1,0:T(8,128)(2,1)} %param.9), channel_id=1, source_target_pairs={{0,8},{8,0},{16,24},{24,16},{1,9},{9,1},{17,25},{25,17},{2,10},{10... | collective-permute-start | bytes 1524104 | tf_op jit(solution)/shard_map/ppermute | solution.py:34
  9.5 2.6 %collective-permute-start.8 = (bf16[256,504]{0,1:T(8,128)(2,1)}, bf16[256,504]{0,1:T(8,128)(2,1)}, u32[]{:S(2)}, u32[]{:S(2)}) collective-permute-start(bf16[256,504]{0,1:T(8,128)(2,1)} %param.6), channel_id=1, source_target_pairs={{0,16},{8,24},{16,0},{24,8},{1,17},{9,25},{17,1},{25,9},{2,18},{10... | collective-permute-start | bytes 774152 | tf_op jit(solution)/shard_map/ppermute | solution.py:25
  12.6 1.5 %fusion.17 = f32[504,504]{1,0:T(8,128)S(1)} fusion(bf16[256,504]{0,1:T(8,128)(2,1)S(1)} %get-tuple-element.11, bf16[256,504]{0,1:T(8,128)(2,1)} %param.6), kind=kOutput, calls=%fused_computation.29 | convolution fusion | flops 130572288 | bytes 1532160 | tf_op jit(solution)/shard_map/dot_general | solution.py:10
  16.5 10.9 %all_gather.11 = bf16[256,1008]{1,0:T(8,128)(2,1)} all-gather(bf16[32,1008]{1,0:T(8,128)(2,1)S(1)} %collective-permute-done.6), channel_id=1, replica_groups=mesh['fs'=4,'tp'=8] {'tp'}, dimensions={0}, use_global_device_ids=true | all-gather | bytes 580608 | tf_op jit(solution)/shard_map/all_gather | solution.py:49
  27.4 9.7 %all_gather.9 = bf16[256,1008]{1,0:T(8,128)(2,1)S(1)} all-gather(bf16[32,1008]{1,0:T(8,128)(2,1)S(1)} %collective-permute-done.1), channel_id=1, replica_groups=mesh['fs'=4,'tp'=8] {'tp'}, dimensions={0}, use_global_device_ids=true | all-gather | bytes 580608 | tf_op jit(solution)/shard_map/all_gather | solution.py:36
  37.1 1.9 %convolution_convert_fusion.2 = bf16[256,504]{0,1:T(8,128)(2,1)S(1)} fusion(bf16[256,1008]{1,0:T(8,128)(2,1)S(1)} %all_gather.9, bf16[504,504]{1,0:T(8,128)(2,1)} %collective-permute-done, bf16[504,504]{1,0:T(8,128)(2,1)} %param.9), kind=kOutput, calls=%fused_computation.13 | convolution fusion | flops 262273536 | bytes 1790208 | tf_op jit(solution)/shard_map/dot_general | solution.py:10
  39.4 2.2 %fusion.3 = bf16[504,504]{1,0:T(8,128)(2,1)} fusion(f32[504,504]{1,0:T(8,128)S(1)} %fusion.17, bf16[256,1008]{1,0:T(8,128)(2,1)S(1)} %all_gather.9, bf16[256,504]{0,1:T(8,128)(2,1)} %collective-permute-done.8), kind=kOutput, calls=%fused_computation.9 | convolution fusion | flops 131080320 | bytes 2060416 | tf_op jit(solution)/shard_map/dot_general | solution.py:10
  41.6 1.6 %collective-permute-start.9 = (bf16[504,504]{1,0:T(8,128)(2,1)}, bf16[504,504]{1,0:T(8,128)(2,1)}, u32[]{:S(2)}, u32[]{:S(2)}) collective-permute-start(bf16[504,504]{1,0:T(8,128)(2,1)} %fusion.3), channel_id=1, source_target_pairs={{0,8},{8,0},{16,24},{24,16},{1,9},{9,1},{17,25},{25,17},{2,10},{10... | collective-permute-start | bytes 1524104 | tf_op jit(solution)/shard_map/ppermute | solution.py:82
  44.3 9.8 %collective-permute-done.2 = bf16[256,504]{0,1:T(8,128)(2,1)S(1)} collective-permute-done((bf16[256,504]{0,1:T(8,128)(2,1)S(1)}, bf16[256,504]{0,1:T(8,128)(2,1)S(1)}, u32[]{:S(2)}, u32[]{:S(2)}) %collective-permute-start.2) | collective-permute-done | bytes 258080 | tf_op jit(solution)/shard_map/ppermute | solution.py:25
  54.1 1.7 %fusion.5 = bf16[256,504]{0,1:T(8,128)(2,1)S(1)} fusion(bf16[504,504]{1,0:T(8,128)(2,1)} %collective-permute-done, bf16[504,504]{1,0:T(8,128)(2,1)} %param.9, bf16[256,504]{0,1:T(8,128)(2,1)S(1)} %copy-done.5, bf16[256,504]{0,1:T(8,128)(2,1)S(1)} %copy-done.3, bf16[256,504]{0,1:T(8,128)(2,1)S(1)} %collective-permute-done.2, bf16[256,504]{0,1:T(8,128)(2,1)} %param.6), kind=kOutput, calls=%fused_computation.12 | convolution fusion | flops 264079872 | bytes 2306304 | tf_op jit(solution)/shard_map/dot_general | solution.py:10
  57.3 3.5 %all-to-all-start.1 = ((bf16[8,32,1008]{2,1,0:T(8,128)(2,1)}), bf16[8,32,1008]{2,1,0:T(8,128)(2,1)S(1)}, u32[]{:S(2)}, u32[]{:S(2)}) async-start(bf16[8,32,1008]{2,1,0:T(8,128)(2,1)} %bitcast.13), calls=%async_computation.1 | async-start | bytes 1048576 | tf_op jit(solution)/shard_map/all_to_all | solution.py:55
  60.8 9.1 %collective-permute-done.3 = bf16[256,504]{0,1:T(8,128)(2,1)S(1)} collective-permute-done((bf16[256,504]{0,1:T(8,128)(2,1)S(1)}, bf16[256,504]{0,1:T(8,128)(2,1)S(1)}, u32[]{:S(2)}, u32[]{:S(2)}) %collective-permute-start.3) | collective-permute-done | bytes 258080 | tf_op jit(solution)/shard_map/ppermute | solution.py:25
  69.9 1.5 %fusion.11 = f32[504,504]{1,0:T(8,128)S(1)} fusion(bf16[256,504]{0,1:T(8,128)(2,1)S(1)} %collective-permute-done.3, bf16[256,1008]{1,0:T(8,128)(2,1)} %all_gather.11), kind=kOutput, calls=%fused_computation.23 | convolution fusion | flops 130056192 | bytes 1536256 | tf_op jit(solution)/shard_map/dot_general | solution.py:10
  71.4 2.1 %fusion.2 = bf16[504,504]{1,0:T(8,128)(2,1)} fusion(f32[504,504]{1,0:T(8,128)S(1)} %fusion.11, bf16[256,504]{0,1:T(8,128)(2,1)S(1)} %fusion.5, bf16[256,2016]{0,1:T(8,128)(2,1)} %param.5, s32[]{:T(128)S(6)} %select_n.100), kind=kOutput, calls=%fused_computation.8 | convolution fusion | flops 130564224 | bytes 2040196 | tf_op jit(solution)/shard_map/dot_general | solution.py:10
  74.7 2.0 %copy.12 = bf16[256,1008]{1,0:T(8,128)(2,1)} copy(bf16[256,1008]{0,1:T(8,128)(2,1)} %convolution_convert_fusion.1) | data formatting | bytes 1032192 | tf_op jit(solution)/shard_map/convert_element_type | solution.py:54
  76.8 4.2 %all-to-all-start = ((bf16[8,32,1008]{2,1,0:T(8,128)(2,1)}), bf16[8,32,1008]{2,1,0:T(8,128)(2,1)}, u32[]{:S(2)}, u32[]{:S(2)}) async-start(bf16[8,32,1008]{2,1,0:T(8,128)(2,1)} %bitcast), calls=%async_computation | async-start | bytes 1048576 | tf_op jit(solution)/shard_map/all_to_all | solution.py:55
  81.0 2.6 %fusion = f32[504,504]{1,0:T(8,128)} fusion(f32[504,504]{1,0:T(8,128)S(1)} %fusion.18, bf16[504,504]{1,0:T(8,128)(2,1)} %collective-permute-done.9, bf16[256,1008]{1,0:T(8,128)(2,1)} %copy-done.1, bf16[256,504]{0,1:T(8,128)(2,1)} %collective-permute-done.8), kind=kOutput, calls=%fused_computation.2 | convolution fusion | flops 131334336 | bytes 3068416 | tf_op jit(solution)/shard_map/dot_general | solution.py:10
  84.0 6.7 %all-to-all-done = bf16[8,32,1008]{2,1,0:T(8,128)(2,1)} async-done(((bf16[8,32,1008]{2,1,0:T(8,128)(2,1)}), bf16[8,32,1008]{2,1,0:T(8,128)(2,1)}, u32[]{:S(2)}, u32[]{:S(2)}) %all-to-all-start) | async-done | bytes 516128 | tf_op jit(solution)/shard_map/all_to_all | solution.py:55
  91.8 2.2 %collective-permute-start.5 = (bf16[32,1008]{1,0:T(8,128)(2,1)S(1)}, bf16[32,1008]{1,0:T(8,128)(2,1)S(1)}, u32[]{:S(2)}, u32[]{:S(2)}) collective-permute-start(bf16[32,1008]{1,0:T(8,128)(2,1)S(1)} %reduce_sum.24), channel_id=1, source_target_pairs={{0,16},{8,24},{16,0},{24,8},{1,17},{9,25},{17,1},{25,9},{2,18},{10... | collective-permute-start | bytes 193544 | tf_op jit(solution)/shard_map/ppermute | solution.py:25
  93.9 2.5 %fusion.1 = f32[504,504]{1,0:T(8,128)} fusion(f32[504,504]{1,0:T(8,128)S(1)} %fusion.13, bf16[256,504]{0,1:T(8,128)(2,1)S(1)} %fusion.5, bf16[504,504]{1,0:T(8,128)(2,1)} %collective-permute-done.7, bf16[256,2016]{0,1:T(8,128)(2,1)} %param.5, s32[]{:T(128)S(6)} %select_n.99), kind=kOutput, calls=%fused_computation.5 | convolution fusion | flops 130818240 | bytes 3064324 | tf_op jit(solution)/shard_map/dot_general | solution.py:10
  97.2 10.7 %all_gather.10 = bf16[256,2016]{1,0:T(8,128)(2,1)S(1)} all-gather(bf16[32,2016]{1,0:T(8,128)(2,1)S(1)} %concatenate.22), channel_id=1, replica_groups=mesh['fs'=4,'tp'=8] {'tp'}, dimensions={0}, use_global_device_ids=true | all-gather | bytes 1161216 | tf_op jit(solution)/shard_map/all_gather | solution.py:67
  107.9 1.3 %copy.16 = bf16[256,2016]{0,1:T(8,128)(2,1)} copy(bf16[256,2016]{1,0:T(8,128)(2,1)S(1)} %all_gather.10) | data formatting | bytes 2064384
  (46 shorter events, 10.8 us)
Async XLA Ops:
  0.6 11.9 %copy-start.6 = (bf16[256,2016]{0,1:T(8,128)(2,1)S(1)}, bf16[256,2016]{0,1:T(8,128)(2,1)}, u32[]{:S(2)}) copy-start(bf16[256,2016]{0,1:T(8,128)(2,1)} %param.7) | copy-start | bytes 3096580
  2.5 14.0 %collective-permute-start.6 = (bf16[32,1008]{1,0:T(8,128)(2,1)S(1)}, bf16[32,1008]{1,0:T(8,128)(2,1)S(1)}, u32[]{:S(2)}, u32[]{:S(2)}) collective-permute-start(bf16[32,1008]{1,0:T(8,128)(2,1)S(1)} %pad_maximum_fusion.4), channel_id=1, source_target_pairs={{0,16},{8,24},{16,0},{24,8},{1,17},{9,25},{17,1},{25,9},{2,18},{10... | collective-permute-start | bytes 193544 | tf_op jit(solution)/shard_map/ppermute | solution.py:25
  7.5 19.8 %collective-permute-start.1 = (bf16[32,1008]{1,0:T(8,128)(2,1)}, bf16[32,1008]{1,0:T(8,128)(2,1)S(1)}, u32[]{:S(2)}, u32[]{:S(2)}) collective-permute-start(bf16[32,1008]{1,0:T(8,128)(2,1)} %pad_maximum_fusion.3), channel_id=1, source_target_pairs={{0,16},{8,24},{16,0},{24,8},{1,17},{9,25},{17,1},{25,9},{2,18},{10... | collective-permute-start | bytes 193544 | tf_op jit(solution)/shard_map/ppermute | solution.py:25
  7.6 29.5 %collective-permute-start = (bf16[504,504]{1,0:T(8,128)(2,1)}, bf16[504,504]{1,0:T(8,128)(2,1)}, u32[]{:S(2)}, u32[]{:S(2)}) collective-permute-start(bf16[504,504]{1,0:T(8,128)(2,1)} %param.9), channel_id=1, source_target_pairs={{0,8},{8,0},{16,24},{24,16},{1,9},{9,1},{17,25},{25,17},{2,10},{10... | collective-permute-start | bytes 1524104 | tf_op jit(solution)/shard_map/ppermute | solution.py:34
  9.5 30.0 %collective-permute-start.8 = (bf16[256,504]{0,1:T(8,128)(2,1)}, bf16[256,504]{0,1:T(8,128)(2,1)}, u32[]{:S(2)}, u32[]{:S(2)}) collective-permute-start(bf16[256,504]{0,1:T(8,128)(2,1)} %param.6), channel_id=1, source_target_pairs={{0,16},{8,24},{16,0},{24,8},{1,17},{9,25},{17,1},{25,9},{2,18},{10... | collective-permute-start | bytes 774152 | tf_op jit(solution)/shard_map/ppermute | solution.py:25
  12.1 31.1 %collective-permute-start.4 = (bf16[504,504]{1,0:T(8,128)(2,1)}, bf16[504,504]{1,0:T(8,128)(2,1)}, u32[]{:S(2)}, u32[]{:S(2)}) collective-permute-start(bf16[504,504]{1,0:T(8,128)(2,1)} %param.8), channel_id=1, source_target_pairs={{0,8},{8,0},{16,24},{24,16},{1,9},{9,1},{17,25},{25,17},{2,10},{10... | collective-permute-start | bytes 1524104 | tf_op jit(solution)/shard_map/ppermute | solution.py:50
  12.5 1.5 %copy-start.4 = (bf16[256,504]{0,1:T(8,128)(2,1)}, bf16[256,504]{0,1:T(8,128)(2,1)S(1)}, u32[]{:S(2)}) copy-start(bf16[256,504]{0,1:T(8,128)(2,1)S(1)} %get-tuple-element.11) | copy-start | bytes 774148
  12.6 2.8 %copy-start.2 = (bf16[256,504]{0,1:T(8,128)(2,1)}, bf16[256,504]{0,1:T(8,128)(2,1)S(1)}, u32[]{:S(2)}) copy-start(bf16[256,504]{0,1:T(8,128)(2,1)S(1)} %get-tuple-element.10) | copy-start | bytes 774148
  37.1 2.3 %copy-start.1 = (bf16[256,1008]{1,0:T(8,128)(2,1)}, bf16[256,1008]{1,0:T(8,128)(2,1)S(1)}, u32[]{:S(2)}) copy-start(bf16[256,1008]{1,0:T(8,128)(2,1)S(1)} %all_gather.9) | copy-start | bytes 1548292
  39.0 15.1 %copy-start.3 = (bf16[256,504]{0,1:T(8,128)(2,1)S(1)}, bf16[256,504]{0,1:T(8,128)(2,1)}, u32[]{:S(2)}) copy-start(bf16[256,504]{0,1:T(8,128)(2,1)} %copy-done.2) | copy-start | bytes 774148
  39.0 15.1 %copy-start.5 = (bf16[256,504]{0,1:T(8,128)(2,1)S(1)}, bf16[256,504]{0,1:T(8,128)(2,1)}, u32[]{:S(2)}) copy-start(bf16[256,504]{0,1:T(8,128)(2,1)} %copy-done.4) | copy-start | bytes 774148
  39.0 15.1 %collective-permute-start.2 = (bf16[256,504]{0,1:T(8,128)(2,1)S(1)}, bf16[256,504]{0,1:T(8,128)(2,1)S(1)}, u32[]{:S(2)}, u32[]{:S(2)}) collective-permute-start(bf16[256,504]{0,1:T(8,128)(2,1)S(1)} %convolution_convert_fusion.2), channel_id=1, source_target_pairs={{0,16},{8,24},{16,0},{24,8},{1,17},{9,25},{17,1},{25,9},{2,18},{10... | collective-permute-start | bytes 774152 | tf_op jit(solution)/shard_map/ppermute | solution.py:25
  41.6 39.4 %collective-permute-start.9 = (bf16[504,504]{1,0:T(8,128)(2,1)}, bf16[504,504]{1,0:T(8,128)(2,1)}, u32[]{:S(2)}, u32[]{:S(2)}) collective-permute-start(bf16[504,504]{1,0:T(8,128)(2,1)} %fusion.3), channel_id=1, source_target_pairs={{0,8},{8,0},{16,24},{24,16},{1,9},{9,1},{17,25},{25,17},{2,10},{10... | collective-permute-start | bytes 1524104 | tf_op jit(solution)/shard_map/ppermute | solution.py:82
  55.8 14.1 %collective-permute-start.3 = (bf16[256,504]{0,1:T(8,128)(2,1)S(1)}, bf16[256,504]{0,1:T(8,128)(2,1)S(1)}, u32[]{:S(2)}, u32[]{:S(2)}) collective-permute-start(bf16[256,504]{0,1:T(8,128)(2,1)S(1)} %fusion.5), channel_id=1, source_target_pairs={{0,16},{8,24},{16,0},{24,8},{1,17},{9,25},{17,1},{25,9},{2,18},{10... | collective-permute-start | bytes 774152 | tf_op jit(solution)/shard_map/ppermute | solution.py:25
  57.3 19.4 %all-to-all-start.1 = ((bf16[8,32,1008]{2,1,0:T(8,128)(2,1)}), bf16[8,32,1008]{2,1,0:T(8,128)(2,1)S(1)}, u32[]{:S(2)}, u32[]{:S(2)}) async-start(bf16[8,32,1008]{2,1,0:T(8,128)(2,1)} %bitcast.13), calls=%async_computation.1 | async-start | bytes 1048576 | tf_op jit(solution)/shard_map/all_to_all | solution.py:55
  73.5 20.5 %collective-permute-start.7 = (bf16[504,504]{1,0:T(8,128)(2,1)}, bf16[504,504]{1,0:T(8,128)(2,1)}, u32[]{:S(2)}, u32[]{:S(2)}) collective-permute-start(bf16[504,504]{1,0:T(8,128)(2,1)} %fusion.2), channel_id=1, source_target_pairs={{0,8},{8,0},{16,24},{24,16},{1,9},{9,1},{17,25},{25,17},{2,10},{10... | collective-permute-start | bytes 1524104 | tf_op jit(solution)/shard_map/ppermute | solution.py:85
  76.8 13.9 %all-to-all-start = ((bf16[8,32,1008]{2,1,0:T(8,128)(2,1)}), bf16[8,32,1008]{2,1,0:T(8,128)(2,1)}, u32[]{:S(2)}, u32[]{:S(2)}) async-start(bf16[8,32,1008]{2,1,0:T(8,128)(2,1)} %bitcast), calls=%async_computation | async-start | bytes 1048576 | tf_op jit(solution)/shard_map/all_to_all | solution.py:55
  80.9 2.6 %copy-start = (bf16[256,1008]{1,0:T(8,128)(2,1)S(1)}, bf16[256,1008]{1,0:T(8,128)(2,1)}, u32[]{:S(2)}) copy-start(bf16[256,1008]{1,0:T(8,128)(2,1)} %all_gather.11) | copy-start | bytes 1548292
  91.8 5.2 %collective-permute-start.5 = (bf16[32,1008]{1,0:T(8,128)(2,1)S(1)}, bf16[32,1008]{1,0:T(8,128)(2,1)S(1)}, u32[]{:S(2)}, u32[]{:S(2)}) collective-permute-start(bf16[32,1008]{1,0:T(8,128)(2,1)S(1)} %reduce_sum.24), channel_id=1, source_target_pairs={{0,16},{8,24},{16,0},{24,8},{1,17},{9,25},{17,1},{25,9},{2,18},{10... | collective-permute-start | bytes 193544 | tf_op jit(solution)/shard_map/ppermute | solution.py:25

commit v2 on v1

v2 whole, which is shorter than its diff:
```python
import jax
import jax.numpy as jnp
from jax import lax
from jax.experimental.layout import Layout, with_layout_constraint
from jax.sharding import PartitionSpec as P

F32, BF16 = jnp.float32, jnp.bfloat16


def dot(a, b, ca, cb):
    return lax.dot_general(a, b, (((ca,), (cb,)), ((), ())), preferred_element_type=F32)


def rows_major(x):
    return with_layout_constraint(x, Layout(major_to_minor=(0, 1)))


def after(x, *deps):
    return lax.optimization_barrier((x, *deps))[0]


def positive(x):
    return jnp.maximum(x.astype(F32), 0.0)


def squared(x):
    return (positive(x) * positive(x)).astype(BF16)


def summed(pairs):
    total = None
    for a, b in pairs:
        term = dot(a, b, 0, 0)
        total = term if total is None else total + term
    return total


def body(inputs, pre_act, cotangent, w_up, w_down, n_fs, n_tp):
    groups = n_fs // 2
    tokens, width = inputs.shape
    block = width // n_fs
    share = tokens // n_tp
    me = lax.axis_index("fs")
    group, side = me // 2, me % 2
    lane = lax.axis_index("tp")
    others = range(1, groups)

    def route(x, k, flip):
        pairs = [(p, (p + 2 * k) % n_fs ^ flip) for p in range(n_fs)]
        return lax.ppermute(x, "fs", pairs)

    def gather(x):
        return lax.all_gather(x, "tp", axis=0, tiled=True)

    def columns(x, row, rows, k, flip):
        at = 2 * ((group + k) % groups) + (side ^ flip)
        return lax.dynamic_slice(x, (row, at * block), (rows, block))

    def both(x, row, rows, k):
        return jnp.concatenate([columns(x, row, rows, k, 0), columns(x, row, rows, k, 1)], axis=1)

    gap = jnp.zeros((share, -2 * block % 128), BF16)
    row = lane * share
    shares = [
        route(jnp.concatenate([both(cotangent, row, share, k), gap, both(inputs, row, share, k)], axis=1), k, 0)
        for k in others
    ]
    w_down_g = jnp.concatenate([w_down, route(w_down, 0, 1)], axis=1)
    w_up_other = route(w_up, 0, 1)
    acts = [route(pre_act, k, 0) for k in others]
    gathered = [gather(s) for s in shares]
    cot = [x[:, : 2 * block] for x in gathered]

    sent = [dot(c, w_down_g, 1, 1).astype(BF16) for c in cot]
    cotangent, inputs, w_up = lax.optimization_barrier((cotangent, inputs, w_up, sent))[:3]
    cot = [both(cotangent, 0, tokens, 0)] + cot
    hidden_grad = lax.optimization_barrier(dot(cot[0], w_down_g, 1, 1))
    for k in others:
        hidden_grad = hidden_grad + route(sent[k - 1], -k, 0).astype(F32)
    pre_grad = [(2.0 * positive(pre_act) * hidden_grad).astype(BF16)]
    pre_grad += [route(pre_grad[0], k, 0) for k in others]
    ins = [both(inputs, 0, tokens, 0)] + [x[:, -2 * block :] for x in gathered]
    w_up_g = jnp.concatenate([w_up, after(w_up_other, pre_grad[0])], axis=0)

    products = []
    for k in range(groups):
        products.append(rows_major(dot(pre_grad[k], w_up_g, 1, 1).astype(BF16)))
    pieces = []
    for k in range(groups):
        terms = after(products[k], pieces[-1]) if k else products[0]
        terms = lax.all_to_all(terms.reshape(n_tp, share, 2 * block), "tp", 0, 0)
        pieces.append(jnp.sum(terms.astype(F32), axis=0).astype(BF16))
    pieces = [pieces[0]] + [route(pieces[k], -k, 0) for k in others]
    ordered = []
    for h in range(groups):
        at = (h - group) % groups
        own, other = pieces[0][:, :block], pieces[0][:, block:]
        for k in others:
            own = jnp.where(at == k, pieces[k][:, :block], own)
            other = jnp.where(at == k, pieces[k][:, block:], other)
        ordered += [jnp.where(side == 0, own, other), jnp.where(side == 0, other, own)]
    grad_input = gather(jnp.concatenate(ordered, axis=1))

    hidden = [squared(a) for a in lax.optimization_barrier(([pre_act] + acts, products[0]))[0]]
    partial = summed([(h, c[:, block:]) for h, c in zip(hidden, cot)]).astype(BF16)
    kept = lax.optimization_barrier(summed([(h, c[:, :block]) for h, c in zip(hidden, cot)]))
    grad_down = kept + route(partial, 0, 1).astype(F32)

    partial = summed([(x[:, block:], p) for x, p in zip(ins, pre_grad)]).astype(BF16)
    kept = lax.optimization_barrier(summed([(x[:, :block], p) for x, p in zip(ins, pre_grad)]))
    received = route(partial, 0, 1)
    grad_up = kept + after(received, grad_input).astype(F32)
    return grad_input, grad_up, grad_down


def solution(mesh):
    n_fs, n_tp = mesh.shape["fs"], mesh.shape["tp"]
    in_specs = (P("fs", None), P("fs", "tp"), P("fs", None), P("fs", "tp"), P("tp", "fs"))
    out_specs = (P("fs", None), P("fs", "tp"), P("tp", "fs"))

    def on_device(*args):
        return body(*args, n_fs, n_tp)

    return jax.shard_map(
        on_device, mesh=mesh, in_specs=in_specs, out_specs=out_specs, check_vma=False
    )
```

time: 110 us -> 107 us (0.973)
  blocking collectives: 31.3 us -> 22.6 us
  waiting for transfers between devices: 26.2 us -> 32.4 us
  other arithmetic: 2.11 us -> 5.71 us
  local copies, waits for them, and re-layouts: 8.61 us -> 5.58 us
  matrix products: 19.1 us -> 16.1 us
  starting transfers between devices: 21 us -> 23 us
    all_gather x3 -> x2, blocking collectives: 31.3 us -> 22.6 us  [gather(): return lax.all_gather(x, 'tp', axis=0, tiled=True)]
    ppermute x10 -> x9, waiting for transfers between devices: 19.5 us -> 25.2 us  [route(): return lax.ppermute(x, 'fs', pairs)]
    add x0 -> x2, other arithmetic: none -> 4.3 us  [the longest x1 2.15 us: body(): grad_down = kept + route(partial, 0, 1).astype(F32)]
    convert_element_type x2 -> x0, local copies, waits for them, and re-layouts: 3.04 us -> none  [body(): terms = dot(pre_grad[k], w_up_g, 1, 1).astype(BF16)]
    dot_general x12, matrix products: 19.1 us -> 16.1 us  [dot(): lax.dot_general(a, b, (((ca,), (cb,)), ((), ())), preferred_element_type=...]
    ppermute x10 -> x9, starting transfers between devices: 13.3 us -> 15.2 us  [route(): return lax.ppermute(x, 'fs', pairs)]
    unnamed x20 -> x14, local copies, waits for them, and re-layouts: 2.92 us -> 2.91 us
  transfers between devices with their start and end apart: 12 -> 11, of which waited for: 4 -> 5; matrix products, arithmetic and copies ran while one was open for 24% -> 23% of each run, Pallas kernels for 0% -> 0%
where the time goes in v2:
time: 107 us; the launch traced here: 106 us
  waiting for transfers between devices  32.4 us (30%)
  starting transfers between devices  23 us (21%)
  blocking collectives  22.6 us (21%)
  matrix products  16.1 us (15%)
  other arithmetic  5.71 us (5%)
  local copies, waits for them, and re-layouts  5.58 us (5%)
    ppermute x9, waiting for transfers between devices, route(): return lax.ppermute(x, 'fs', pairs)  25.2 us
    all_gather x2, blocking collectives, gather(): return lax.all_gather(x, 'tp', axis=0, tiled=True)  22.6 us
    dot_general x12, matrix products, dot(): lax.dot_general(a, b, (((ca,), (cb,)), ((), ())), preferred_element_type=...  16.1 us
    ppermute x9, starting transfers between devices, route(): return lax.ppermute(x, 'fs', pairs)  15.2 us
    all_to_all x2, starting transfers between devices, body(): terms = lax.all_to_all(terms.reshape(n_tp, share, 2 * block), 'tp', 0, 0)  7.86 us
    all_to_all x2, waiting for transfers between devices, body(): terms = lax.all_to_all(terms.reshape(n_tp, share, 2 * block), 'tp', 0, 0)  7.13 us
    unnamed x14, local copies, waits for them, and re-layouts  2.91 us
    add x1, other arithmetic, body(): grad_down = kept + route(partial, 0, 1).astype(F32)  2.15 us
  transfers between devices with their start and end apart: 11, of which 5 were waited for; matrix products, arithmetic and copies ran while one was open for 23% of the time, Pallas kernels for 0%

profile of v2, /device:TPU:0, one launch (start us, length us, event | category | flops | bytes accessed | tf_op | source)
XLA Modules:
  0.0 106.1 jit_solution(2376263749640010022)
XLA Ops:
  0.6 3.1 %collective-permute-start.1 = (bf16[504,504]{1,0:T(8,128)(2,1)}, bf16[504,504]{1,0:T(8,128)(2,1)}, u32[]{:S(2)}, u32[]{:S(2)}) collective-permute-start(bf16[504,504]{1,0:T(8,128)(2,1)} %param.9), channel_id=1, source_target_pairs={{0,8},{8,0},{16,24},{24,16},{1,9},{9,1},{17,25},{25,17},{2,10},{10... | collective-permute-start | bytes 1524104 | tf_op jit(solution)/shard_map/ppermute | solution.py:50
  3.8 1.3 %fusion.25 = (bf16[32,504]{0,1:T(8,128)(2,1)S(1)}, bf16[32,504]{0,1:T(8,128)(2,1)S(1)}, bf16[32,504]{0,1:T(8,128)(2,1)S(1)}, bf16[32,504]{0,1:T(8,128)(2,1)S(1)}) fusion(bf16[256,2016]{0,1:T(8,128)(2,1)} %param.5, s32[]{:T(128)S(6)} %select_n.106, s32[]{:T(128)S(6)} %select_n.109, s32[]{:T(128)S(6)} %select_n.108, bf16[256,2016]{0,1:T(8,128)(2,1)} %param.7), kind=kLoop, calls=%fused_computation.50 | loop fusion | bytes 258060 | tf_op jit(solution)/shard_map/dynamic_slice | solution.py:57
  5.7 2.7 %collective-permute-start = (bf16[32,2032]{1,0:T(8,128)(2,1)S(1)}, bf16[32,2032]{1,0:T(8,128)(2,1)S(1)}, u32[]{:S(2)}, u32[]{:S(2)}) collective-permute-start(bf16[32,2032]{1,0:T(8,128)(2,1)S(1)} %concatenate.15), channel_id=1, source_target_pairs={{0,16},{8,24},{16,0},{24,8},{1,17},{9,25},{17,1},{25,9},{2,18},{10... | collective-permute-start | bytes 390152 | tf_op jit(solution)/shard_map/ppermute | solution.py:50
  8.9 10.0 %collective-permute-done = bf16[32,2032]{1,0:T(8,128)(2,1)S(1)} collective-permute-done((bf16[32,2032]{1,0:T(8,128)(2,1)S(1)}, bf16[32,2032]{1,0:T(8,128)(2,1)S(1)}, u32[]{:S(2)}, u32[]{:S(2)}) %collective-permute-start) | collective-permute-done | bytes 130080 | tf_op jit(solution)/shard_map/ppermute | solution.py:50
  18.9 11.1 %all_gather.6 = bf16[256,2032]{1,0:T(8,128)(2,1)S(1)} all-gather(bf16[32,2032]{1,0:T(8,128)(2,1)S(1)} %collective-permute-done), channel_id=1, replica_groups=mesh['fs'=4,'tp'=8] {'tp'}, dimensions={0}, use_global_device_ids=true | all-gather | bytes 1170432 | tf_op jit(solution)/shard_map/all_gather | solution.py:53
  30.1 1.8 %convolution_convert_fusion.2 = bf16[256,504]{0,1:T(8,128)(2,1)S(1)} fusion(bf16[504,504]{1,0:T(8,128)(2,1)} %collective-permute-done.1, bf16[504,504]{1,0:T(8,128)(2,1)} %param.9, bf16[256,2032]{1,0:T(8,128)(2,1)S(1)} %all_gather.6), kind=kOutput, calls=%fused_computation.8 | convolution fusion | flops 262273536 | bytes 1798400 | tf_op jit(solution)/shard_map/dot_general | solution.py:11
  31.9 3.4 %collective-permute-start.2 = (bf16[256,504]{0,1:T(8,128)(2,1)S(1)}, bf16[256,504]{0,1:T(8,128)(2,1)S(1)}, u32[]{:S(2)}, u32[]{:S(2)}) collective-permute-start(bf16[256,504]{0,1:T(8,128)(2,1)S(1)} %convolution_convert_fusion.2), channel_id=1, source_target_pairs={{0,16},{8,24},{16,0},{24,8},{1,17},{9,25},{17,1},{25,9},{2,18},{10... | collective-permute-start | bytes 774152 | tf_op jit(solution)/shard_map/ppermute | solution.py:50
  35.4 1.5 %fusion.2 = f32[256,504]{0,1:T(8,128)S(1)} fusion(bf16[504,504]{1,0:T(8,128)(2,1)} %collective-permute-done.1, bf16[504,504]{1,0:T(8,128)(2,1)S(1)} %copy-done.3, bf16[256,504]{0,1:T(8,128)(2,1)S(1)} %get-tuple-element.23, bf16[256,504]{0,1:T(8,128)(2,1)S(1)} %get-tuple-element.22), kind=kOutput, calls=%fused_computation.12 | convolution fusion | flops 263176704 | bytes 2048256 | tf_op jit(solution)/shard_map/dot_general | solution.py:11
  38.0 10.4 %collective-permute-done.2 = bf16[256,504]{0,1:T(8,128)(2,1)S(1)} collective-permute-done((bf16[256,504]{0,1:T(8,128)(2,1)S(1)}, bf16[256,504]{0,1:T(8,128)(2,1)S(1)}, u32[]{:S(2)}, u32[]{:S(2)}) %collective-permute-start.2) | collective-permute-done | bytes 258080 | tf_op jit(solution)/shard_map/ppermute | solution.py:50
  49.6 1.3 %convolution_convert_fusion = bf16[256,1008]{1,0:T(8,128)(2,1)} fusion(bf16[256,504]{0,1:T(8,128)(2,1)S(1)} %multiply_convert_fusion.2, bf16[1008,504]{1,0:T(8,128)(2,1)S(1)} %constant_dynamic-update-slice_fusion), kind=kOutput, calls=%fused_computation.4 | convolution fusion | flops 260370432 | bytes 1790208 | tf_op jit(solution)/shard_map/dot_general | solution.py:11
  52.8 2.2 %collective-permute-start.8 = (bf16[504,504]{1,0:T(8,128)(2,1)}, bf16[504,504]{1,0:T(8,128)(2,1)}, u32[]{:S(2)}, u32[]{:S(2)}) collective-permute-start(bf16[504,504]{1,0:T(8,128)(2,1)} %fusion.1), channel_id=1, source_target_pairs={{0,8},{8,0},{16,24},{24,16},{1,9},{9,1},{17,25},{25,17},{2,10},{10... | collective-permute-start | bytes 1524104 | tf_op jit(solution)/shard_map/ppermute | solution.py:50
  56.3 4.2 %all-to-all-start = ((bf16[8,32,1008]{2,1,0:T(8,128)(2,1)}), bf16[8,32,1008]{2,1,0:T(8,128)(2,1)}, u32[]{:S(2)}, u32[]{:S(2)}) async-start(bf16[8,32,1008]{2,1,0:T(8,128)(2,1)} %bitcast.12), calls=%async_computation | async-start | bytes 1048576 | tf_op jit(solution)/shard_map/all_to_all | solution.py:91
  60.5 4.7 %collective-permute-done.3 = bf16[256,504]{0,1:T(8,128)(2,1)} collective-permute-done((bf16[256,504]{0,1:T(8,128)(2,1)S(1)}, bf16[256,504]{0,1:T(8,128)(2,1)}, u32[]{:S(2)}, u32[]{:S(2)}) %collective-permute-start.3) | collective-permute-done | bytes 258080 | tf_op jit(solution)/shard_map/ppermute | solution.py:50
  65.2 1.4 %fusion.9 = f32[504,504]{1,0:T(8,128)S(1)} fusion(bf16[256,504]{0,1:T(8,128)(2,1)} %collective-permute-done.3, bf16[256,2032]{1,0:T(8,128)(2,1)S(1)} %all_gather.6), kind=kOutput, calls=%fused_computation.22 | convolution fusion | flops 130056192 | bytes 1536256 | tf_op jit(solution)/shard_map/dot_general | solution.py:11
  66.6 2.1 %fusion = bf16[504,504]{1,0:T(8,128)(2,1)} fusion(f32[504,504]{1,0:T(8,128)S(1)} %fusion.9, bf16[256,504]{0,1:T(8,128)(2,1)S(1)} %multiply_convert_fusion.2, bf16[256,2016]{0,1:T(8,128)(2,1)} %param.5, s32[]{:T(128)S(6)} %select_n.112), kind=kOutput, calls=%fused_computation.6 | convolution fusion | flops 130564224 | bytes 2040196 | tf_op jit(solution)/shard_map/dot_general | solution.py:11
  68.7 2.2 %convolution_convert_fusion.1 = bf16[256,1008]{1,0:T(8,128)(2,1)} fusion(bf16[256,504]{0,1:T(8,128)(2,1)} %collective-permute-done.3, bf16[1008,504]{1,0:T(8,128)(2,1)S(1)} %constant_dynamic-update-slice_fusion), kind=kOutput, calls=%fused_computation.5 | convolution fusion | flops 260370432 | bytes 1790208 | tf_op jit(solution)/shard_map/dot_general | solution.py:11
  72.1 3.7 %all-to-all-start.1 = ((bf16[8,32,1008]{2,1,0:T(8,128)(2,1)}), bf16[8,32,1008]{2,1,0:T(8,128)(2,1)S(1)}, u32[]{:S(2)}, u32[]{:S(2)}) async-start(bf16[8,32,1008]{2,1,0:T(8,128)(2,1)} %bitcast.13), calls=%async_computation.1 | async-start | bytes 1048576 | tf_op jit(solution)/shard_map/all_to_all | solution.py:91
  75.8 1.3 %fusion.11 = f32[504,504]{1,0:T(8,128)S(1)} fusion(bf16[256,504]{0,1:T(8,128)(2,1)} %collective-permute-done.3, bf16[256,2032]{1,0:T(8,128)(2,1)S(1)} %all_gather.6), kind=kOutput, calls=%fused_computation.24 | convolution fusion | flops 130056192 | bytes 1536256 | tf_op jit(solution)/shard_map/dot_general | solution.py:11
  78.4 7.1 %all-to-all-done.1 = bf16[8,32,1008]{2,1,0:T(8,128)(2,1)S(1)} async-done(((bf16[8,32,1008]{2,1,0:T(8,128)(2,1)}), bf16[8,32,1008]{2,1,0:T(8,128)(2,1)S(1)}, u32[]{:S(2)}, u32[]{:S(2)}) %all-to-all-start.1) | async-done | bytes 516128 | tf_op jit(solution)/shard_map/all_to_all | solution.py:91
  85.6 3.1 %collective-permute-start.5 = (bf16[32,1008]{1,0:T(8,128)(2,1)S(1)}, bf16[32,1008]{1,0:T(8,128)(2,1)S(1)}, u32[]{:S(2)}, u32[]{:S(2)}) collective-permute-start(bf16[32,1008]{1,0:T(8,128)(2,1)S(1)} %reduce_sum.25), channel_id=1, source_target_pairs={{0,16},{8,24},{16,0},{24,8},{1,17},{9,25},{17,1},{25,9},{2,18},{10... | collective-permute-start | bytes 193544 | tf_op jit(solution)/shard_map/ppermute | solution.py:50
  88.7 2.1 %convert_add_fusion = f32[504,504]{1,0:T(8,128)} fusion(f32[504,504]{1,0:T(8,128)S(1)} %convolution_add_fusion.1, bf16[504,504]{1,0:T(8,128)(2,1)} %collective-permute-done.8), kind=kLoop, calls=%fused_computation.10 | loop fusion | flops 508032 | bytes 2540160 | tf_op jit(solution)/shard_map/add | solution.py:107
  91.2 11.5 %all_gather.7 = bf16[256,2016]{1,0:T(8,128)(2,1)S(1)} all-gather(bf16[32,2016]{1,0:T(8,128)(2,1)S(1)} %concatenate.19), channel_id=1, replica_groups=mesh['fs'=4,'tp'=8] {'tp'}, dimensions={0}, use_global_device_ids=true | all-gather | bytes 1161216 | tf_op jit(solution)/shard_map/all_gather | solution.py:53
  102.7 1.3 %copy.12 = bf16[256,2016]{0,1:T(8,128)(2,1)} copy(bf16[256,2016]{1,0:T(8,128)(2,1)S(1)} %all_gather.7) | data formatting | bytes 2064384
  104.0 2.1 %convert_add_fusion.1 = f32[504,504]{1,0:T(8,128)} fusion(f32[504,504]{1,0:T(8,128)S(1)} %convolution_add_fusion.3, bf16[504,504]{1,0:T(8,128)(2,1)} %collective-permute-done.6), kind=kLoop, calls=%fused_computation.11 | loop fusion | flops 508032 | bytes 2540160 | tf_op jit(solution)/shard_map/add | solution.py:112
  (38 shorter events, 9.4 us)
Async XLA Ops:
  0.6 8.2 %copy-start = (bf16[256,504]{0,1:T(8,128)(2,1)S(1)}, bf16[256,504]{0,1:T(8,128)(2,1)}, u32[]{:S(2)}) copy-start(bf16[256,504]{0,1:T(8,128)(2,1)} %param.6) | copy-start | bytes 774148
  0.6 29.4 %collective-permute-start.1 = (bf16[504,504]{1,0:T(8,128)(2,1)}, bf16[504,504]{1,0:T(8,128)(2,1)}, u32[]{:S(2)}, u32[]{:S(2)}) collective-permute-start(bf16[504,504]{1,0:T(8,128)(2,1)} %param.9), channel_id=1, source_target_pairs={{0,8},{8,0},{16,24},{24,16},{1,9},{9,1},{17,25},{25,17},{2,10},{10... | collective-permute-start | bytes 1524104 | tf_op jit(solution)/shard_map/ppermute | solution.py:50
  5.7 13.2 %collective-permute-start = (bf16[32,2032]{1,0:T(8,128)(2,1)S(1)}, bf16[32,2032]{1,0:T(8,128)(2,1)S(1)}, u32[]{:S(2)}, u32[]{:S(2)}) collective-permute-start(bf16[32,2032]{1,0:T(8,128)(2,1)S(1)} %concatenate.15), channel_id=1, source_target_pairs={{0,16},{8,24},{16,0},{24,8},{1,17},{9,25},{17,1},{25,9},{2,18},{10... | collective-permute-start | bytes 390152 | tf_op jit(solution)/shard_map/ppermute | solution.py:50
  8.4 40.1 %collective-permute-start.4 = (bf16[504,504]{1,0:T(8,128)(2,1)}, bf16[504,504]{1,0:T(8,128)(2,1)}, u32[]{:S(2)}, u32[]{:S(2)}) collective-permute-start(bf16[504,504]{1,0:T(8,128)(2,1)} %param.8), channel_id=1, source_target_pairs={{0,8},{8,0},{16,24},{24,16},{1,9},{9,1},{17,25},{25,17},{2,10},{10... | collective-permute-start | bytes 1524104 | tf_op jit(solution)/shard_map/ppermute | solution.py:50
  8.8 42.0 %collective-permute-start.7 = (bf16[256,504]{0,1:T(8,128)(2,1)S(1)}, bf16[256,504]{0,1:T(8,128)(2,1)S(1)}, u32[]{:S(2)}, u32[]{:S(2)}) collective-permute-start(bf16[256,504]{0,1:T(8,128)(2,1)S(1)} %copy-done), channel_id=1, source_target_pairs={{0,16},{8,24},{16,0},{24,8},{1,17},{9,25},{17,1},{25,9},{2,18},{10... | collective-permute-start | bytes 774152 | tf_op jit(solution)/shard_map/ppermute | solution.py:50
  30.1 5.3 %copy-start.2 = (bf16[256,2016]{0,1:T(8,128)(2,1)S(1)}, bf16[256,2016]{0,1:T(8,128)(2,1)}, u32[]{:S(2)}) copy-start(bf16[256,2016]{0,1:T(8,128)(2,1)} %param.7) | copy-start | bytes 3096580
  30.1 5.3 %copy-start.3 = (bf16[504,504]{1,0:T(8,128)(2,1)S(1)}, bf16[504,504]{1,0:T(8,128)(2,1)}, u32[]{:S(2)}) copy-start(bf16[504,504]{1,0:T(8,128)(2,1)} %param.9) | copy-start | bytes 1524100
  31.9 16.5 %collective-permute-start.2 = (bf16[256,504]{0,1:T(8,128)(2,1)S(1)}, bf16[256,504]{0,1:T(8,128)(2,1)S(1)}, u32[]{:S(2)}, u32[]{:S(2)}) collective-permute-start(bf16[256,504]{0,1:T(8,128)(2,1)S(1)} %convolution_convert_fusion.2), channel_id=1, source_target_pairs={{0,16},{8,24},{16,0},{24,8},{1,17},{9,25},{17,1},{25,9},{2,18},{10... | collective-permute-start | bytes 774152 | tf_op jit(solution)/shard_map/ppermute | solution.py:50
  50.9 2.0 %copy-start.1 = (bf16[256,504]{0,1:T(8,128)(2,1)}, bf16[256,504]{0,1:T(8,128)(2,1)S(1)}, u32[]{:S(2)}) copy-start(bf16[256,504]{0,1:T(8,128)(2,1)S(1)} %collective-permute-done.7) | copy-start | bytes 774148
  51.5 13.7 %collective-permute-start.3 = (bf16[256,504]{0,1:T(8,128)(2,1)S(1)}, bf16[256,504]{0,1:T(8,128)(2,1)}, u32[]{:S(2)}, u32[]{:S(2)}) collective-permute-start(bf16[256,504]{0,1:T(8,128)(2,1)S(1)} %multiply_convert_fusion.2), channel_id=1, source_target_pairs={{0,16},{8,24},{16,0},{24,8},{1,17},{9,25},{17,1},{25,9},{2,18},{10... | collective-permute-start | bytes 774152 | tf_op jit(solution)/shard_map/ppermute | solution.py:50
  52.8 35.9 %collective-permute-start.8 = (bf16[504,504]{1,0:T(8,128)(2,1)}, bf16[504,504]{1,0:T(8,128)(2,1)}, u32[]{:S(2)}, u32[]{:S(2)}) collective-permute-start(bf16[504,504]{1,0:T(8,128)(2,1)} %fusion.1), channel_id=1, source_target_pairs={{0,8},{8,0},{16,24},{24,16},{1,9},{9,1},{17,25},{25,17},{2,10},{10... | collective-permute-start | bytes 1524104 | tf_op jit(solution)/shard_map/ppermute | solution.py:50
  56.3 14.7 %all-to-all-start = ((bf16[8,32,1008]{2,1,0:T(8,128)(2,1)}), bf16[8,32,1008]{2,1,0:T(8,128)(2,1)}, u32[]{:S(2)}, u32[]{:S(2)}) async-start(bf16[8,32,1008]{2,1,0:T(8,128)(2,1)} %bitcast.12), calls=%async_computation | async-start | bytes 1048576 | tf_op jit(solution)/shard_map/all_to_all | solution.py:91
  68.7 35.3 %collective-permute-start.6 = (bf16[504,504]{1,0:T(8,128)(2,1)}, bf16[504,504]{1,0:T(8,128)(2,1)}, u32[]{:S(2)}, u32[]{:S(2)}) collective-permute-start(bf16[504,504]{1,0:T(8,128)(2,1)} %fusion), channel_id=1, source_target_pairs={{0,8},{8,0},{16,24},{24,16},{1,9},{9,1},{17,25},{25,17},{2,10},{10... | collective-permute-start | bytes 1524104 | tf_op jit(solution)/shard_map/ppermute | solution.py:50
  72.1 13.4 %all-to-all-start.1 = ((bf16[8,32,1008]{2,1,0:T(8,128)(2,1)}), bf16[8,32,1008]{2,1,0:T(8,128)(2,1)S(1)}, u32[]{:S(2)}, u32[]{:S(2)}) async-start(bf16[8,32,1008]{2,1,0:T(8,128)(2,1)} %bitcast.13), calls=%async_computation.1 | async-start | bytes 1048576 | tf_op jit(solution)/shard_map/all_to_all | solution.py:91
  85.6 5.3 %collective-permute-start.5 = (bf16[32,1008]{1,0:T(8,128)(2,1)S(1)}, bf16[32,1008]{1,0:T(8,128)(2,1)S(1)}, u32[]{:S(2)}, u32[]{:S(2)}) collective-permute-start(bf16[32,1008]{1,0:T(8,128)(2,1)S(1)} %reduce_sum.25), channel_id=1, source_target_pairs={{0,16},{8,24},{16,0},{24,8},{1,17},{9,25},{17,1},{25,9},{2,18},{10... | collective-permute-start | bytes 193544 | tf_op jit(solution)/shard_map/ppermute | solution.py:50

commit v3 on v2

--- a/solution.py
+++ b/solution.py
@@ -59,27 +59,33 @@
     def both(x, row, rows, k):
         return jnp.concatenate([columns(x, row, rows, k, 0), columns(x, row, rows, k, 1)], axis=1)
 
-    gap = jnp.zeros((share, -2 * block % 128), BF16)
     row = lane * share
-    shares = [
-        route(jnp.concatenate([both(cotangent, row, share, k), gap, both(inputs, row, share, k)], axis=1), k, 0)
-        for k in others
-    ]
-    w_down_g = jnp.concatenate([w_down, route(w_down, 0, 1)], axis=1)
+    cot_shares = [route(both(cotangent, row, share, k), k, 0) for k in others]
+    w_down_other = route(w_down, 0, 1)
+    in_shares = [route(both(inputs, row, share, k), k, 0) for k in others]
+    cot = [gather(s) for s in cot_shares]
+    w_down_g = jnp.concatenate([w_down, w_down_other], axis=1)
     w_up_other = route(w_up, 0, 1)
     acts = [route(pre_act, k, 0) for k in others]
-    gathered = [gather(s) for s in shares]
-    cot = [x[:, : 2 * block] for x in gathered]
 
-    sent = [dot(c, w_down_g, 1, 1).astype(BF16) for c in cot]
-    cotangent, inputs, w_up = lax.optimization_barrier((cotangent, inputs, w_up, sent))[:3]
+    units = pre_act.shape[1]
+    half = (units // 2 + 15) // 16 * 16
+    runs = [slice(0, half), slice(half, units)]
+    sent = [[dot(c, w_down_g[run], 1, 1).astype(BF16) for c in cot] for run in runs]
+    cotangent, inputs, w_up, late = lax.optimization_barrier((cotangent, inputs, w_up, in_shares, sent))[:4]
     cot = [both(cotangent, 0, tokens, 0)] + cot
-    hidden_grad = lax.optimization_barrier(dot(cot[0], w_down_g, 1, 1))
-    for k in others:
-        hidden_grad = hidden_grad + route(sent[k - 1], -k, 0).astype(F32)
-    pre_grad = [(2.0 * positive(pre_act) * hidden_grad).astype(BF16)]
-    pre_grad += [route(pre_grad[0], k, 0) for k in others]
-    ins = [both(inputs, 0, tokens, 0)] + [x[:, -2 * block :] for x in gathered]
+    pre_grad = []
+    for n, run in enumerate(runs):
+        hidden_grad = lax.optimization_barrier(dot(cot[0], w_down_g[run], 1, 1))
+        for k in others:
+            hidden_grad = hidden_grad + route(sent[n][k - 1], -k, 0).astype(F32)
+        pre_grad.append((2.0 * positive(pre_act[:, run]) * hidden_grad).astype(BF16))
+    pre_grad = [pre_grad] + [[route(p, k, 0) for p in pre_grad] for k in others]
+    pre_grad = [jnp.concatenate(p, axis=1) for p in pre_grad]
+    ins = [both(inputs, 0, tokens, 0)]
+    for x in late:
+        x = lax.all_to_all(jnp.broadcast_to(x, (n_tp, *x.shape)), "tp", 0, 0)
+        ins.append(x.reshape(tokens, 2 * block))
     w_up_g = jnp.concatenate([w_up, after(w_up_other, pre_grad[0])], axis=0)
 
     products = []
@@ -87,9 +93,16 @@
         products.append(rows_major(dot(pre_grad[k], w_up_g, 1, 1).astype(BF16)))
     pieces = []
     for k in range(groups):
-        terms = after(products[k], pieces[-1]) if k else products[0]
-        terms = lax.all_to_all(terms.reshape(n_tp, share, 2 * block), "tp", 0, 0)
-        pieces.append(jnp.sum(terms.astype(F32), axis=0).astype(BF16))
+        halves = products[k].reshape(n_tp // 2, 2, share, 2 * block)
+        give = lax.dynamic_index_in_dim(halves, 1 - lane % 2, 1, keepdims=False)
+        keep = lax.dynamic_index_in_dim(halves, lane % 2, 1, keepdims=False)
+        taken = lax.ppermute(give, "tp", [(t, t ^ 1) for t in range(n_tp)])
+        pieces.append((keep.astype(F32) + taken.astype(F32)).astype(BF16))
+    same_parity = [list(range(c, n_tp, 2)) for c in (0, 1)]
+    terms = after(jnp.concatenate(pieces, axis=1), ins[1:])
+    terms = lax.all_to_all(terms, "tp", 0, 0, axis_index_groups=same_parity)
+    terms = [terms[:, k * share : (k + 1) * share] for k in range(groups)]
+    pieces = [jnp.sum(t.astype(F32), axis=0).astype(BF16) for t in terms]
     pieces = [pieces[0]] + [route(pieces[k], -k, 0) for k in others]
     ordered = []
     for h in range(groups):

time: 107 us -> 105 us (0.981)
  waiting for transfers between devices: 32.4 us -> 25.1 us
  other arithmetic: 5.71 us -> 10.3 us
  local copies, waits for them, and re-layouts: 5.58 us -> 8.37 us
  blocking collectives: 22.6 us -> 21 us
  matrix products: 16.1 us -> 14.7 us
    ppermute x9 -> x12, waiting for transfers between devices: 25.2 us -> 19.4 us  [route(): return lax.ppermute(x, 'fs', pairs)]
    convert_element_type x1 -> x4, other arithmetic: 0.11 us -> 3.79 us  [the longest x2 1.94 us: body(): (2.0 * positive(pre_act[:, run]) * hidden_grad).astype(BF16)]
    all_gather x2, blocking collectives: 22.6 us -> 21 us  [gather(): return lax.all_gather(x, 'tp', axis=0, tiled=True)]
    all_to_all x2, waiting for transfers between devices: 7.13 us -> 5.71 us  [the longest x1 5.71 us: body(): terms = lax.all_to_all(terms, 'tp', 0, 0, axis_index_groups=same_parity)]
    dot_general x12 -> x14, matrix products: 16.1 us -> 14.7 us  [dot(): lax.dot_general(a, b, (((ca,), (cb,)), ((), ())), preferred_element_type=...]
    unnamed x14 -> x35, local copies, waits for them, and re-layouts: 2.91 us -> 4.04 us
    ppermute x9 -> x12, starting transfers between devices: 15.2 us -> 14.7 us  [route(): return lax.ppermute(x, 'fs', pairs)]
  transfers between devices with their start and end apart: 11 -> 16, of which waited for: 5 -> 6; matrix products, arithmetic and copies ran while one was open for 23% -> 29% of each run, Pallas kernels for 0% -> 0%
where the time goes in v3:
time: 105 us; the launch traced here: 104 us
  waiting for transfers between devices  25.1 us (24%)
  starting transfers between devices  23.2 us (22%)
  blocking collectives  21 us (20%)
  matrix products  14.7 us (14%)
  other arithmetic  10.3 us (10%)
  local copies, waits for them, and re-layouts  8.37 us (8%)
  between operations  1.12 us (1%)
    all_gather x2, blocking collectives, gather(): return lax.all_gather(x, 'tp', axis=0, tiled=True)  21 us
    ppermute x12, waiting for transfers between devices, route(): return lax.ppermute(x, 'fs', pairs)  19.4 us
    ppermute x12, starting transfers between devices, route(): return lax.ppermute(x, 'fs', pairs)  14.7 us
    dot_general x14, matrix products, dot(): lax.dot_general(a, b, (((ca,), (cb,)), ((), ())), preferred_element_type=...  14.7 us
    all_to_all x1, waiting for transfers between devices, body(): terms = lax.all_to_all(terms, 'tp', 0, 0, axis_index_groups=same_parity)  5.71 us
    all_to_all x1, starting transfers between devices, body(): terms = lax.all_to_all(terms, 'tp', 0, 0, axis_index_groups=same_parity)  4.27 us
    all_to_all x1, starting transfers between devices, body(): x = lax.all_to_all(jnp.broadcast_to(x, (n_tp, *x.shape)), 'tp', 0, 0)  4.14 us
    unnamed x35, local copies, waits for them, and re-layouts  4.04 us
  transfers between devices with their start and end apart: 16, of which 6 were waited for; matrix products, arithmetic and copies ran while one was open for 29% of the time, Pallas kernels for 0%

profile of v3, /device:TPU:0, one launch (start us, length us, event | category | flops | bytes accessed | tf_op | source)
XLA Modules:
  0.0 103.7 jit_solution(17454406946975516337)
XLA Ops:
  0.6 3.1 %collective-permute-start.2 = (bf16[504,504]{1,0:T(8,128)(2,1)}, bf16[504,504]{1,0:T(8,128)(2,1)S(1)}, u32[]{:S(2)}, u32[]{:S(2)}) collective-permute-start(bf16[504,504]{1,0:T(8,128)(2,1)} %param.9), channel_id=1, source_target_pairs={{0,8},{8,0},{16,24},{24,16},{1,9},{9,1},{17,25},{25,17},{2,10},{10... | collective-permute-start | bytes 1524104 | tf_op jit(solution)/shard_map/ppermute | solution.py:50
  3.7 1.3 %fusion.28 = (bf16[32,504]{0,1:T(8,128)(2,1)S(1)}, bf16[32,504]{0,1:T(8,128)(2,1)S(1)}, bf16[32,504]{0,1:T(8,128)(2,1)S(1)}, bf16[32,504]{0,1:T(8,128)(2,1)S(1)}) fusion(bf16[256,2016]{0,1:T(8,128)(2,1)} %param.7, s32[]{:T(128)S(6)} %select_n.125, s32[]{:T(128)S(6)} %select_n.127, s32[]{:T(128)S(6)} %select_n.128, bf16[256,2016]{0,1:T(8,128)(2,1)} %param.5), kind=kLoop, calls=%fused_computation.68 | loop fusion | bytes 258060 | tf_op jit(solution)/shard_map/dynamic_slice | solution.py:57
  5.4 2.7 %collective-permute-start.1 = (bf16[32,1008]{1,0:T(8,128)(2,1)S(1)}, bf16[32,1008]{1,0:T(8,128)(2,1)S(1)}, u32[]{:S(2)}, u32[]{:S(2)}) collective-permute-start(bf16[32,1008]{1,0:T(8,128)(2,1)S(1)} %pad_maximum_fusion.7), channel_id=1, source_target_pairs={{0,16},{8,24},{16,0},{24,8},{1,17},{9,25},{17,1},{25,9},{2,18},{10... | collective-permute-start | bytes 193544 | tf_op jit(solution)/shard_map/ppermute | solution.py:50
  9.0 2.8 %collective-permute-start.12 = (bf16[256,504]{0,1:T(8,128)(2,1)S(1)}, bf16[256,504]{0,1:T(8,128)(2,1)}, u32[]{:S(2)}, u32[]{:S(2)}) collective-permute-start(bf16[256,504]{0,1:T(8,128)(2,1)S(1)} %copy-done), channel_id=1, source_target_pairs={{0,16},{8,24},{16,0},{24,8},{1,17},{9,25},{17,1},{25,9},{2,18},{10... | collective-permute-start | bytes 774152 | tf_op jit(solution)/shard_map/ppermute | solution.py:50
  12.2 5.3 %collective-permute-done.1 = bf16[32,1008]{1,0:T(8,128)(2,1)S(1)} collective-permute-done((bf16[32,1008]{1,0:T(8,128)(2,1)S(1)}, bf16[32,1008]{1,0:T(8,128)(2,1)S(1)}, u32[]{:S(2)}, u32[]{:S(2)}) %collective-permute-start.1) | collective-permute-done | bytes 64544 | tf_op jit(solution)/shard_map/ppermute | solution.py:50
  17.5 9.8 %all_gather.6 = bf16[256,1008]{1,0:T(8,128)(2,1)S(1)} all-gather(bf16[32,1008]{1,0:T(8,128)(2,1)S(1)} %collective-permute-done.1), channel_id=1, replica_groups=mesh['fs'=4,'tp'=8] {'tp'}, dimensions={0}, use_global_device_ids=true | all-gather | bytes 580608 | tf_op jit(solution)/shard_map/all_gather | solution.py:53
  28.4 3.4 %collective-permute-start.4 = (bf16[256,248]{1,0:T(8,128)(2,1)}, bf16[256,248]{1,0:T(8,128)(2,1)}, u32[]{:S(2)}, u32[]{:S(2)}) collective-permute-start(bf16[256,248]{1,0:T(8,128)(2,1)} %convolution_convert_fusion.2), channel_id=1, source_target_pairs={{0,16},{8,24},{16,0},{24,8},{1,17},{9,25},{17,1},{25,9},{2,18},{10... | collective-permute-start | bytes 380936 | tf_op jit(solution)/shard_map/ppermute | solution.py:50
  36.6 4.1 %all-to-all-start = ((bf16[8,32,1008]{2,1,0:T(8,128)(2,1)}), bf16[8,32,1008]{2,1,0:T(8,128)(2,1)}, u32[]{:S(2)}, u32[]{:S(2)}) async-start(bf16[8,32,1008]{2,1,0:T(8,128)(2,1)} %broadcast_in_dim.3), calls=%async_computation | async-start | bytes 1048576 | tf_op jit(solution)/shard_map/all_to_all | solution.py:87
  41.8 4.0 %collective-permute-done.4 = bf16[256,248]{1,0:T(8,128)(2,1)} collective-permute-done((bf16[256,248]{1,0:T(8,128)(2,1)}, bf16[256,248]{1,0:T(8,128)(2,1)}, u32[]{:S(2)}, u32[]{:S(2)}) %collective-permute-start.4) | collective-permute-done | bytes 127008 | tf_op jit(solution)/shard_map/ppermute | solution.py:50
  46.9 1.7 %collective-permute-done.3 = bf16[256,256]{1,0:T(8,128)(2,1)} collective-permute-done((bf16[256,256]{1,0:T(8,128)(2,1)}, bf16[256,256]{1,0:T(8,128)(2,1)}, u32[]{:S(2)}, u32[]{:S(2)}) %collective-permute-start.3) | collective-permute-done | bytes 131104 | tf_op jit(solution)/shard_map/ppermute | solution.py:50
  50.1 1.4 %fusion.7 = f32[504,504]{1,0:T(8,128)S(1)} fusion(bf16[256,1008]{1,0:T(8,128)(2,1)S(1)} %all_gather.6, bf16[256,504]{0,1:T(8,128)(2,1)} %collective-permute-done.12), kind=kOutput, calls=%fused_computation.26 | convolution fusion | flops 130572288 | bytes 1536256 | tf_op jit(solution)/shard_map/dot_general | solution.py:11
  51.5 1.3 %fusion.9 = f32[504,504]{1,0:T(8,128)S(1)} fusion(bf16[256,1008]{1,0:T(8,128)(2,1)S(1)} %all_gather.6, bf16[256,504]{0,1:T(8,128)(2,1)} %collective-permute-done.12), kind=kOutput, calls=%fused_computation.28 | convolution fusion | flops 130572288 | bytes 1536256 | tf_op jit(solution)/shard_map/dot_general | solution.py:11
  56.3 5.1 %collective-permute-done.7 = bf16[256,256]{1,0:T(8,128)(2,1)S(1)} collective-permute-done((bf16[256,256]{1,0:T(8,128)(2,1)S(1)}, bf16[256,256]{1,0:T(8,128)(2,1)S(1)}, u32[]{:S(2)}, u32[]{:S(2)}) %collective-permute-start.7) | collective-permute-done | bytes 131104 | tf_op jit(solution)/shard_map/ppermute | solution.py:50
  64.3 1.4 %fusion.11 = f32[504,504]{1,0:T(8,128)S(1)} fusion(bf16[256,504]{1,0:T(8,128)(2,1)S(1)} %constant_dynamic-update-slice_fusion.2, bf16[256,1008]{1,0:T(8,128)(2,1)} %bitcast.6), kind=kOutput, calls=%fused_computation.30 | convolution fusion | flops 130056192 | bytes 1536256 | tf_op jit(solution)/shard_map/dot_general | solution.py:11
  65.7 1.3 %fusion.13 = f32[504,504]{1,0:T(8,128)S(1)} fusion(bf16[256,504]{1,0:T(8,128)(2,1)S(1)} %constant_dynamic-update-slice_fusion.2, bf16[256,1008]{1,0:T(8,128)(2,1)} %bitcast.6), kind=kOutput, calls=%fused_computation.32 | convolution fusion | flops 130056192 | bytes 1536256 | tf_op jit(solution)/shard_map/dot_general | solution.py:11
  69.0 4.3 %all-to-all-start.1 = ((bf16[4,64,1008]{2,1,0:T(8,128)(2,1)}), bf16[4,64,1008]{2,1,0:T(8,128)(2,1)}, u32[]{:S(2)}, u32[]{:S(2)}) async-start(bf16[4,64,1008]{2,1,0:T(8,128)(2,1)} %pad_maximum_fusion), calls=%async_computation.1 | async-start | bytes 1048576 | tf_op jit(solution)/shard_map/all_to_all | solution.py:103
  73.3 2.0 %fusion = bf16[504,504]{1,0:T(8,128)(2,1)} fusion(f32[504,504]{1,0:T(8,128)S(1)} %fusion.11, bf16[256,2016]{0,1:T(8,128)(2,1)} %param.5, s32[]{:T(128)S(6)} %select_n.131, bf16[256,248]{1,0:T(8,128)(2,1)S(1)} %multiply_convert_fusion.2, bf16[256,256]{1,0:T(8,128)(2,1)S(1)} %copy-done.2), kind=kOutput, calls=%fused_computation.6 | convolution fusion | flops 131080320 | bytes 2040196 | tf_op jit(solution)/shard_map/dot_general | solution.py:11
  75.4 1.2 %convolution_add_fusion.3 = f32[504,504]{1,0:T(8,128)S(1)} fusion(f32[504,504]{1,0:T(8,128)S(1)} %fusion.13, bf16[256,2016]{0,1:T(8,128)(2,1)} %param.5, s32[]{:T(128)S(6)} %select_n.130, bf16[256,248]{1,0:T(8,128)(2,1)S(1)} %multiply_convert_fusion.2, bf16[256,256]{1,0:T(8,128)(2,1)S(1)} %copy-done.2), kind=kOutput, calls=%fused_computation.3 | convolution fusion | flops 130826304 | bytes 2548228 | tf_op jit(solution)/shard_map/dot_general | solution.py:11
  76.6 5.7 %all-to-all-done.1 = bf16[4,64,1008]{2,1,0:T(8,128)(2,1)} async-done(((bf16[4,64,1008]{2,1,0:T(8,128)(2,1)}), bf16[4,64,1008]{2,1,0:T(8,128)(2,1)}, u32[]{:S(2)}, u32[]{:S(2)}) %all-to-all-start.1) | async-done | bytes 516128 | tf_op jit(solution)/shard_map/all_to_all | solution.py:103
  83.5 2.1 %convert_add_fusion = f32[504,504]{1,0:T(8,128)} fusion(f32[504,504]{1,0:T(8,128)S(1)} %convolution_add_fusion.1, bf16[504,504]{1,0:T(8,128)(2,1)} %collective-permute-done.13), kind=kLoop, calls=%fused_computation.12 | loop fusion | flops 508032 | bytes 2540160 | tf_op jit(solution)/shard_map/add | solution.py:120
  85.7 3.2 %collective-permute-done.10 = bf16[32,1008]{1,0:T(8,128)(2,1)S(1)} collective-permute-done((bf16[32,1008]{1,0:T(8,128)(2,1)S(1)}, bf16[32,1008]{1,0:T(8,128)(2,1)S(1)}, u32[]{:S(2)}, u32[]{:S(2)}) %collective-permute-start.10) | collective-permute-done | bytes 64544 | tf_op jit(solution)/shard_map/ppermute | solution.py:50
  89.1 11.1 %all_gather.7 = bf16[256,2016]{1,0:T(8,128)(2,1)S(1)} all-gather(bf16[32,2016]{1,0:T(8,128)(2,1)S(1)} %concatenate.35), channel_id=1, replica_groups=mesh['fs'=4,'tp'=8] {'tp'}, dimensions={0}, use_global_device_ids=true | all-gather | bytes 1161216 | tf_op jit(solution)/shard_map/all_gather | solution.py:53
  100.2 1.3 %copy.24 = bf16[256,2016]{0,1:T(8,128)(2,1)} copy(bf16[256,2016]{1,0:T(8,128)(2,1)S(1)} %all_gather.7) | data formatting | bytes 2064384
  101.6 2.1 %convert_add_fusion.1 = f32[504,504]{1,0:T(8,128)} fusion(f32[504,504]{1,0:T(8,128)S(1)} %convolution_add_fusion.3, bf16[504,504]{1,0:T(8,128)(2,1)} %collective-permute-done.11), kind=kLoop, calls=%fused_computation.13 | loop fusion | flops 508032 | bytes 2540160 | tf_op jit(solution)/shard_map/add | solution.py:125
  (81 shorter events, 20.5 us)
Async XLA Ops:
  0.6 26.7 %collective-permute-start.2 = (bf16[504,504]{1,0:T(8,128)(2,1)}, bf16[504,504]{1,0:T(8,128)(2,1)S(1)}, u32[]{:S(2)}, u32[]{:S(2)}) collective-permute-start(bf16[504,504]{1,0:T(8,128)(2,1)} %param.9), channel_id=1, source_target_pairs={{0,8},{8,0},{16,24},{24,16},{1,9},{9,1},{17,25},{25,17},{2,10},{10... | collective-permute-start | bytes 1524104 | tf_op jit(solution)/shard_map/ppermute | solution.py:50
  5.4 3.6 %copy-start = (bf16[256,504]{0,1:T(8,128)(2,1)S(1)}, bf16[256,504]{0,1:T(8,128)(2,1)}, u32[]{:S(2)}) copy-start(bf16[256,504]{0,1:T(8,128)(2,1)} %param.6) | copy-start | bytes 774148
  5.4 12.1 %collective-permute-start.1 = (bf16[32,1008]{1,0:T(8,128)(2,1)S(1)}, bf16[32,1008]{1,0:T(8,128)(2,1)S(1)}, u32[]{:S(2)}, u32[]{:S(2)}) collective-permute-start(bf16[32,1008]{1,0:T(8,128)(2,1)S(1)} %pad_maximum_fusion.7), channel_id=1, source_target_pairs={{0,16},{8,24},{16,0},{24,8},{1,17},{9,25},{17,1},{25,9},{2,18},{10... | collective-permute-start | bytes 193544 | tf_op jit(solution)/shard_map/ppermute | solution.py:50
  8.4 24.4 %collective-permute-start = (bf16[32,1008]{1,0:T(8,128)(2,1)S(1)}, bf16[32,1008]{1,0:T(8,128)(2,1)S(1)}, u32[]{:S(2)}, u32[]{:S(2)}) collective-permute-start(bf16[32,1008]{1,0:T(8,128)(2,1)S(1)} %pad_maximum_fusion.6), channel_id=1, source_target_pairs={{0,16},{8,24},{16,0},{24,8},{1,17},{9,25},{17,1},{25,9},{2,18},{10... | collective-permute-start | bytes 193544 | tf_op jit(solution)/shard_map/ppermute | solution.py:50
  8.8 26.9 %collective-permute-start.5 = (bf16[504,504]{1,0:T(8,128)(2,1)}, bf16[504,504]{1,0:T(8,128)(2,1)}, u32[]{:S(2)}, u32[]{:S(2)}) collective-permute-start(bf16[504,504]{1,0:T(8,128)(2,1)} %param.8), channel_id=1, source_target_pairs={{0,8},{8,0},{16,24},{24,16},{1,9},{9,1},{17,25},{25,17},{2,10},{10... | collective-permute-start | bytes 1524104 | tf_op jit(solution)/shard_map/ppermute | solution.py:50
  9.0 41.1 %collective-permute-start.12 = (bf16[256,504]{0,1:T(8,128)(2,1)S(1)}, bf16[256,504]{0,1:T(8,128)(2,1)}, u32[]{:S(2)}, u32[]{:S(2)}) collective-permute-start(bf16[256,504]{0,1:T(8,128)(2,1)S(1)} %copy-done), channel_id=1, source_target_pairs={{0,16},{8,24},{16,0},{24,8},{1,17},{9,25},{17,1},{25,9},{2,18},{10... | collective-permute-start | bytes 774152 | tf_op jit(solution)/shard_map/ppermute | solution.py:50
  11.9 15.4 %copy-start.9 = (bf16[504,504]{1,0:T(8,128)(2,1)S(1)}, bf16[504,504]{1,0:T(8,128)(2,1)}, u32[]{:S(2)}) copy-start(bf16[504,504]{1,0:T(8,128)(2,1)} %param.9) | copy-start | bytes 1524100
  27.3 5.6 %copy-start.10 = (bf16[504,504]{1,0:T(8,128)(2,1)}, bf16[504,504]{1,0:T(8,128)(2,1)S(1)}, u32[]{:S(2)}) copy-start(bf16[504,504]{1,0:T(8,128)(2,1)S(1)} %collective-permute-done.2) | copy-start | bytes 1524100
  28.4 4.4 %copy-start.8 = (bf16[256,2016]{0,1:T(8,128)(2,1)S(1)}, bf16[256,2016]{0,1:T(8,128)(2,1)}, u32[]{:S(2)}) copy-start(bf16[256,2016]{0,1:T(8,128)(2,1)} %param.7) | copy-start | bytes 3096580
  28.4 17.4 %collective-permute-start.4 = (bf16[256,248]{1,0:T(8,128)(2,1)}, bf16[256,248]{1,0:T(8,128)(2,1)}, u32[]{:S(2)}, u32[]{:S(2)}) collective-permute-start(bf16[256,248]{1,0:T(8,128)(2,1)} %convolution_convert_fusion.2), channel_id=1, source_target_pairs={{0,16},{8,24},{16,0},{24,8},{1,17},{9,25},{17,1},{25,9},{2,18},{10... | collective-permute-start | bytes 380936 | tf_op jit(solution)/shard_map/ppermute | solution.py:50
  32.8 15.8 %collective-permute-start.3 = (bf16[256,256]{1,0:T(8,128)(2,1)}, bf16[256,256]{1,0:T(8,128)(2,1)}, u32[]{:S(2)}, u32[]{:S(2)}) collective-permute-start(bf16[256,256]{1,0:T(8,128)(2,1)} %convolution_convert_fusion.3), channel_id=1, source_target_pairs={{0,16},{8,24},{16,0},{24,8},{1,17},{9,25},{17,1},{25,9},{2,18},{10... | collective-permute-start | bytes 393224 | tf_op jit(solution)/shard_map/ppermute | solution.py:50
  36.6 27.7 %all-to-all-start = ((bf16[8,32,1008]{2,1,0:T(8,128)(2,1)}), bf16[8,32,1008]{2,1,0:T(8,128)(2,1)}, u32[]{:S(2)}, u32[]{:S(2)}) async-start(bf16[8,32,1008]{2,1,0:T(8,128)(2,1)} %broadcast_in_dim.3), calls=%async_computation | async-start | bytes 1048576 | tf_op jit(solution)/shard_map/all_to_all | solution.py:87
  41.8 6.8 %copy-start.12 = (f32[256,256]{1,0:T(8,128)S(1)}, f32[256,256]{1,0:T(8,128)}, u32[]{:S(2)}) copy-start(f32[256,256]{1,0:T(8,128)} %fusion.6) | copy-start | bytes 786436
  46.8 14.7 %collective-permute-start.8 = (bf16[256,248]{1,0:T(8,128)(2,1)S(1)}, bf16[256,248]{1,0:T(8,128)(2,1)S(1)}, u32[]{:S(2)}, u32[]{:S(2)}) collective-permute-start(bf16[256,248]{1,0:T(8,128)(2,1)S(1)} %multiply_convert_fusion.2), channel_id=1, source_target_pairs={{0,16},{8,24},{16,0},{24,8},{1,17},{9,25},{17,1},{25,9},{2,18},{10... | collective-permute-start | bytes 380936 | tf_op jit(solution)/shard_map/ppermute | solution.py:50
  49.6 3.2 %copy-start.1 = (bf16[256,256]{1,0:T(8,128)(2,1)}, bf16[256,256]{1,0:T(8,128)(2,1)S(1)}, u32[]{:S(2)}) copy-start(bf16[256,256]{1,0:T(8,128)(2,1)S(1)} %multiply_convert_fusion.3) | copy-start | bytes 393220
  51.5 2.6 %copy-start.7 = (bf16[256,504]{0,1:T(8,128)(2,1)S(1)}, bf16[256,504]{0,1:T(8,128)(2,1)}, u32[]{:S(2)}) copy-start(bf16[256,504]{0,1:T(8,128)(2,1)} %copy-done.6) | copy-start | bytes 774148
  52.8 8.7 %collective-permute-start.7 = (bf16[256,256]{1,0:T(8,128)(2,1)S(1)}, bf16[256,256]{1,0:T(8,128)(2,1)S(1)}, u32[]{:S(2)}, u32[]{:S(2)}) collective-permute-start(bf16[256,256]{1,0:T(8,128)(2,1)S(1)} %multiply_convert_fusion.3), channel_id=1, source_target_pairs={{0,16},{8,24},{16,0},{24,8},{1,17},{9,25},{17,1},{25,9},{2,18},{10... | collective-permute-start | bytes 393224 | tf_op jit(solution)/shard_map/ppermute | solution.py:50
  55.2 28.4 %collective-permute-start.13 = (bf16[504,504]{1,0:T(8,128)(2,1)}, bf16[504,504]{1,0:T(8,128)(2,1)}, u32[]{:S(2)}, u32[]{:S(2)}) collective-permute-start(bf16[504,504]{1,0:T(8,128)(2,1)} %fusion.1), channel_id=1, source_target_pairs={{0,8},{8,0},{16,24},{24,16},{1,9},{9,1},{17,25},{25,17},{2,10},{10... | collective-permute-start | bytes 1524104 | tf_op jit(solution)/shard_map/ppermute | solution.py:50
  56.3 7.2 %collective-permute-start.6 = (bf16[4,32,1008]{2,1,0:T(8,128)(2,1)S(1)}, bf16[4,32,1008]{2,1,0:T(8,128)(2,1)S(1)}, u32[]{:S(2)}, u32[]{:S(2)}) collective-permute-start(bf16[4,32,1008]{2,1,0:T(8,128)(2,1)S(1)} %dynamic-slice_bitcast_fusion.1), channel_id=1, source_target_pairs={{0,1},{1,0},{2,3},{3,2},{4,5},{5,4},{6,7},{7,6},{8,9},{9,8},{10,11... | collective-permute-start | bytes 774152 | tf_op jit(solution)/shard_map/ppermute | solution.py:99
  63.5 3.6 %collective-permute-start.9 = (bf16[4,32,1008]{2,1,0:T(8,128)(2,1)}, bf16[4,32,1008]{2,1,0:T(8,128)(2,1)}, u32[]{:S(2)}, u32[]{:S(2)}) collective-permute-start(bf16[4,32,1008]{2,1,0:T(8,128)(2,1)} %dynamic-slice_bitcast_fusion), channel_id=1, source_target_pairs={{0,1},{1,0},{2,3},{3,2},{4,5},{5,4},{6,7},{7,6},{8,9},{9,8},{10,11... | collective-permute-start | bytes 774152 | tf_op jit(solution)/shard_map/ppermute | solution.py:99
  69.0 4.3 %copy-start.2 = (bf16[256,256]{1,0:T(8,128)(2,1)S(1)}, bf16[256,256]{1,0:T(8,128)(2,1)}, u32[]{:S(2)}) copy-start(bf16[256,256]{1,0:T(8,128)(2,1)} %copy-done.1) | copy-start | bytes 393220
  69.0 13.3 %all-to-all-start.1 = ((bf16[4,64,1008]{2,1,0:T(8,128)(2,1)}), bf16[4,64,1008]{2,1,0:T(8,128)(2,1)}, u32[]{:S(2)}, u32[]{:S(2)}) async-start(bf16[4,64,1008]{2,1,0:T(8,128)(2,1)} %pad_maximum_fusion), calls=%async_computation.1 | async-start | bytes 1048576 | tf_op jit(solution)/shard_map/all_to_all | solution.py:103
  75.3 26.2 %collective-permute-start.11 = (bf16[504,504]{1,0:T(8,128)(2,1)}, bf16[504,504]{1,0:T(8,128)(2,1)}, u32[]{:S(2)}, u32[]{:S(2)}) collective-permute-start(bf16[504,504]{1,0:T(8,128)(2,1)} %fusion), channel_id=1, source_target_pairs={{0,8},{8,0},{16,24},{24,16},{1,9},{9,1},{17,25},{25,17},{2,10},{10... | collective-permute-start | bytes 1524104 | tf_op jit(solution)/shard_map/ppermute | solution.py:50
  83.4 5.5 %collective-permute-start.10 = (bf16[32,1008]{1,0:T(8,128)(2,1)S(1)}, bf16[32,1008]{1,0:T(8,128)(2,1)S(1)}, u32[]{:S(2)}, u32[]{:S(2)}) collective-permute-start(bf16[32,1008]{1,0:T(8,128)(2,1)S(1)} %get-tuple-element.24), channel_id=1, source_target_pairs={{0,16},{8,24},{16,0},{24,8},{1,17},{9,25},{17,1},{25,9},{2,18},{10... | collective-permute-start | bytes 193544 | tf_op jit(solution)/shard_map/ppermute | solution.py:50
  (5 other events, 6.8 us)

commit v4 on v3

--- a/solution.py
+++ b/solution.py
@@ -59,20 +59,25 @@
     def both(x, row, rows, k):
         return jnp.concatenate([columns(x, row, rows, k, 0), columns(x, row, rows, k, 1)], axis=1)
 
+    gap = jnp.zeros((share, -2 * block % 128), BF16)
     row = lane * share
-    cot_shares = [route(both(cotangent, row, share, k), k, 0) for k in others]
+    shares = [
+        route(jnp.concatenate([both(cotangent, row, share, k), gap, both(inputs, row, share, k)], axis=1), k, 0)
+        for k in others
+    ]
     w_down_other = route(w_down, 0, 1)
-    in_shares = [route(both(inputs, row, share, k), k, 0) for k in others]
-    cot = [gather(s) for s in cot_shares]
+    gathered = [gather(s) for s in shares]
+    cot = [x[:, : 2 * block] for x in gathered]
     w_down_g = jnp.concatenate([w_down, w_down_other], axis=1)
-    w_up_other = route(w_up, 0, 1)
+    cut = block // 32 * 16
+    w_up_parts = [route(w_up[:cut], 0, 1), route(w_up[cut:], 0, 1)]
     acts = [route(pre_act, k, 0) for k in others]
 
     units = pre_act.shape[1]
     half = (units // 2 + 15) // 16 * 16
     runs = [slice(0, half), slice(half, units)]
     sent = [[dot(c, w_down_g[run], 1, 1).astype(BF16) for c in cot] for run in runs]
-    cotangent, inputs, w_up, late = lax.optimization_barrier((cotangent, inputs, w_up, in_shares, sent))[:4]
+    cotangent, inputs, w_up = lax.optimization_barrier((cotangent, inputs, w_up, sent))[:3]
     cot = [both(cotangent, 0, tokens, 0)] + cot
     pre_grad = []
     for n, run in enumerate(runs):
@@ -82,11 +87,8 @@
         pre_grad.append((2.0 * positive(pre_act[:, run]) * hidden_grad).astype(BF16))
     pre_grad = [pre_grad] + [[route(p, k, 0) for p in pre_grad] for k in others]
     pre_grad = [jnp.concatenate(p, axis=1) for p in pre_grad]
-    ins = [both(inputs, 0, tokens, 0)]
-    for x in late:
-        x = lax.all_to_all(jnp.broadcast_to(x, (n_tp, *x.shape)), "tp", 0, 0)
-        ins.append(x.reshape(tokens, 2 * block))
-    w_up_g = jnp.concatenate([w_up, after(w_up_other, pre_grad[0])], axis=0)
+    ins = [both(inputs, 0, tokens, 0)] + [x[:, -2 * block :] for x in gathered]
+    w_up_g = jnp.concatenate([w_up, *after(w_up_parts, pre_grad[0])], axis=0)
 
     products = []
     for k in range(groups):
@@ -99,7 +101,7 @@
         taken = lax.ppermute(give, "tp", [(t, t ^ 1) for t in range(n_tp)])
         pieces.append((keep.astype(F32) + taken.astype(F32)).astype(BF16))
     same_parity = [list(range(c, n_tp, 2)) for c in (0, 1)]
-    terms = after(jnp.concatenate(pieces, axis=1), ins[1:])
+    terms = jnp.concatenate(pieces, axis=1)
     terms = lax.all_to_all(terms, "tp", 0, 0, axis_index_groups=same_parity)
     terms = [terms[:, k * share : (k + 1) * share] for k in range(groups)]
     pieces = [jnp.sum(t.astype(F32), axis=0).astype(BF16) for t in terms]
@@ -114,7 +116,7 @@
         ordered += [jnp.where(side == 0, own, other), jnp.where(side == 0, other, own)]
     grad_input = gather(jnp.concatenate(ordered, axis=1))
 
-    hidden = [squared(a) for a in lax.optimization_barrier(([pre_act] + acts, products[0]))[0]]
+    hidden = [squared(a) for a in lax.optimization_barrier(([pre_act] + acts, pre_grad[0]))[0]]
     partial = summed([(h, c[:, block:]) for h, c in zip(hidden, cot)]).astype(BF16)
     kept = lax.optimization_barrier(summed([(h, c[:, :block]) for h, c in zip(hidden, cot)]))
     grad_down = kept + route(partial, 0, 1).astype(F32)

time: 105 us -> 102 us (0.971)
  matrix products: 14.7 us -> 10.5 us
  other arithmetic: 10.3 us -> 6.62 us
  starting transfers between devices: 23.2 us -> 25.9 us
  local copies, waits for them, and re-layouts: 8.37 us -> 10.6 us
    ppermute x12, starting transfers between devices: 14.7 us -> 21.1 us  [route(): return lax.ppermute(x, 'fs', pairs)]
    dot_general x14, matrix products: 14.7 us -> 10.5 us  [dot(): lax.dot_general(a, b, (((ca,), (cb,)), ((), ())), preferred_element_type=...]
    all_to_all x1 -> x0, starting transfers between devices: 4.14 us -> none  [body(): x = lax.all_to_all(jnp.broadcast_to(x, (n_tp, *x.shape)), 'tp', 0, 0)]
    convert_element_type x2, other arithmetic: 1.94 us -> 0.14 us  [body(): (2.0 * positive(pre_act[:, run]) * hidden_grad).astype(BF16)]
    ppermute x12, waiting for transfers between devices: 19.4 us -> 17.6 us  [route(): return lax.ppermute(x, 'fs', pairs)]
    convert_element_type x2, other arithmetic: 1.86 us -> 0.14 us  [body(): pieces.append((keep.astype(F32) + taken.astype(F32)).astype(BF16))]
    all_to_all x1, waiting for transfers between devices: 5.71 us -> 7.3 us  [body(): terms = lax.all_to_all(terms, 'tp', 0, 0, axis_index_groups=same_parity)]
    slice x0 -> x2, local copies, waits for them, and re-layouts: none -> 1.43 us  [body(): w_up_parts = [route(w_up[:cut], 0, 1), route(w_up[cut:], 0, 1)]]
  transfers between devices with their start and end apart: 16 -> 15, of which waited for: 6 -> 7; matrix products, arithmetic and copies ran while one was open for 29% -> 23% of each run, Pallas kernels for 0% -> 0%
where the time goes in v4:
time: 102 us
  starting transfers between devices  25.9 us (25%)
  waiting for transfers between devices  25.7 us (25%)
  blocking collectives  21.2 us (21%)
  local copies, waits for them, and re-layouts  10.6 us (10%)
  matrix products  10.5 us (10%)
  other arithmetic  6.62 us (6%)
  between operations  1.05 us (1%)
    all_gather x2, blocking collectives, gather(): return lax.all_gather(x, 'tp', axis=0, tiled=True)  21.2 us
    ppermute x12, starting transfers between devices, route(): return lax.ppermute(x, 'fs', pairs)  21.1 us
    ppermute x12, waiting for transfers between devices, route(): return lax.ppermute(x, 'fs', pairs)  17.6 us
    dot_general x14, matrix products, dot(): lax.dot_general(a, b, (((ca,), (cb,)), ((), ())), preferred_element_type=...  10.5 us
    all_to_all x1, waiting for transfers between devices, body(): terms = lax.all_to_all(terms, 'tp', 0, 0, axis_index_groups=same_parity)  7.3 us
    unnamed x32, local copies, waits for them, and re-layouts  5.4 us
    all_to_all x1, starting transfers between devices, body(): terms = lax.all_to_all(terms, 'tp', 0, 0, axis_index_groups=same_parity)  4.13 us
    add x1, other arithmetic, body(): grad_down = kept + route(partial, 0, 1).astype(F32)  2.15 us
  transfers between devices with their start and end apart: 15, of which 7 were waited for; matrix products, arithmetic and copies ran while one was open for 23% of the time, Pallas kernels for 0%

profile of v4, /device:TPU:0, one launch (start us, length us, event | category | flops | bytes accessed | tf_op | source)
XLA Modules:
  0.0 101.5 jit_solution(18434959935439184020)
XLA Ops:
  0.6 3.1 %collective-permute-start.1 = (bf16[504,504]{1,0:T(8,128)(2,1)}, bf16[504,504]{1,0:T(8,128)(2,1)S(1)}, u32[]{:S(2)}, u32[]{:S(2)}) collective-permute-start(bf16[504,504]{1,0:T(8,128)(2,1)} %param.9), channel_id=1, source_target_pairs={{0,8},{8,0},{16,24},{24,16},{1,9},{9,1},{17,25},{25,17},{2,10},{10... | collective-permute-start | bytes 1524104 | tf_op jit(solution)/shard_map/ppermute | solution.py:50
  3.7 1.3 %fusion.30 = (bf16[32,504]{0,1:T(8,128)(2,1)S(1)}, bf16[32,504]{0,1:T(8,128)(2,1)S(1)}, bf16[32,504]{0,1:T(8,128)(2,1)S(1)}, bf16[32,504]{0,1:T(8,128)(2,1)S(1)}) fusion(bf16[256,2016]{0,1:T(8,128)(2,1)} %param.5, s32[]{:T(128)S(6)} %select_n.125, s32[]{:T(128)S(6)} %select_n.128, s32[]{:T(128)S(6)} %select_n.127, bf16[256,2016]{0,1:T(8,128)(2,1)} %param.7), kind=kLoop, calls=%fused_computation.69 | loop fusion | bytes 258060 | tf_op jit(solution)/shard_map/dynamic_slice | solution.py:57
  5.7 2.7 %collective-permute-start = (bf16[32,2032]{1,0:T(8,128)(2,1)S(1)}, bf16[32,2032]{1,0:T(8,128)(2,1)S(1)}, u32[]{:S(2)}, u32[]{:S(2)}) collective-permute-start(bf16[32,2032]{1,0:T(8,128)(2,1)S(1)} %concatenate.24), channel_id=1, source_target_pairs={{0,16},{8,24},{16,0},{24,8},{1,17},{9,25},{17,1},{25,9},{2,18},{10... | collective-permute-start | bytes 390152 | tf_op jit(solution)/shard_map/ppermute | solution.py:50
  10.9 1.6 %collective-permute-start.4 = (bf16[240,504]{1,0:T(8,128)(2,1)}, bf16[240,504]{1,0:T(8,128)(2,1)}, u32[]{:S(2)}, u32[]{:S(2)}) collective-permute-start(bf16[240,504]{1,0:T(8,128)(2,1)} %slice.67), channel_id=1, source_target_pairs={{0,8},{8,0},{16,24},{24,16},{1,9},{9,1},{17,25},{25,17},{2,10},{10... | collective-permute-start | bytes 725768 | tf_op jit(solution)/shard_map/ppermute | solution.py:50
  12.8 6.1 %collective-permute-done = bf16[32,2032]{1,0:T(8,128)(2,1)S(1)} collective-permute-done((bf16[32,2032]{1,0:T(8,128)(2,1)S(1)}, bf16[32,2032]{1,0:T(8,128)(2,1)S(1)}, u32[]{:S(2)}, u32[]{:S(2)}) %collective-permute-start) | collective-permute-done | bytes 130080 | tf_op jit(solution)/shard_map/ppermute | solution.py:50
  18.9 11.0 %all_gather.6 = bf16[256,2032]{1,0:T(8,128)(2,1)S(1)} all-gather(bf16[32,2032]{1,0:T(8,128)(2,1)S(1)} %collective-permute-done), channel_id=1, replica_groups=mesh['fs'=4,'tp'=8] {'tp'}, dimensions={0}, use_global_device_ids=true | all-gather | bytes 1170432 | tf_op jit(solution)/shard_map/all_gather | solution.py:53
  31.0 3.4 %collective-permute-start.3 = (bf16[256,248]{1,0:T(8,128)(2,1)}, bf16[256,248]{1,0:T(8,128)(2,1)S(1)}, u32[]{:S(2)}, u32[]{:S(2)}) collective-permute-start(bf16[256,248]{1,0:T(8,128)(2,1)} %convolution_convert_fusion.2), channel_id=1, source_target_pairs={{0,16},{8,24},{16,0},{24,8},{1,17},{9,25},{17,1},{25,9},{2,18},{10... | collective-permute-start | bytes 380936 | tf_op jit(solution)/shard_map/ppermute | solution.py:50
  34.5 1.0 %convolution_convert_fusion.3 = bf16[256,256]{1,0:T(8,128)(2,1)} fusion(bf16[256,2032]{1,0:T(8,128)(2,1)S(1)} %all_gather.6, bf16[504,504]{1,0:T(8,128)(2,1)S(1)} %copy-done.7, bf16[504,504]{1,0:T(8,128)(2,1)S(1)} %collective-permute-done.1), kind=kOutput, calls=%fused_computation.9 | convolution fusion | flops 133218304 | bytes 1687552 | tf_op jit(solution)/shard_map/dot_general | solution.py:11
  36.6 1.2 %fusion.8 = f32[256,256]{1,0:T(8,128)} fusion(bf16[256,504]{0,1:T(8,128)(2,1)S(1)} %get-tuple-element.25, bf16[256,504]{0,1:T(8,128)(2,1)S(1)} %get-tuple-element.24, bf16[504,504]{1,0:T(8,128)(2,1)S(1)} %copy-done.7, bf16[504,504]{1,0:T(8,128)(2,1)S(1)} %copy-done.9), kind=kOutput, calls=%fused_computation.27 | convolution fusion | flops 134184960 | bytes 1794304 | tf_op jit(solution)/shard_map/dot_general | solution.py:11
  38.8 1.1 %copy.20 = f32[256,248]{1,0:T(8,128)S(1)} copy(f32[256,248]{0,1:T(8,128)} %fusion.7) | data formatting | bytes 507904 | tf_op jit(solution)/shard_map/optimization_barrier | solution.py:84
  39.9 4.8 %collective-permute-done.3 = bf16[256,248]{1,0:T(8,128)(2,1)S(1)} collective-permute-done((bf16[256,248]{1,0:T(8,128)(2,1)}, bf16[256,248]{1,0:T(8,128)(2,1)S(1)}, u32[]{:S(2)}, u32[]{:S(2)}) %collective-permute-start.3) | collective-permute-done | bytes 127008 | tf_op jit(solution)/shard_map/ppermute | solution.py:50
  44.8 2.3 %collective-permute-done.2 = bf16[256,256]{1,0:T(8,128)(2,1)S(1)} collective-permute-done((bf16[256,256]{1,0:T(8,128)(2,1)}, bf16[256,256]{1,0:T(8,128)(2,1)S(1)}, u32[]{:S(2)}, u32[]{:S(2)}) %collective-permute-start.2) | collective-permute-done | bytes 131104 | tf_op jit(solution)/shard_map/ppermute | solution.py:50
  49.9 1.2 %fusion.1 = bf16[504,504]{1,0:T(8,128)(2,1)} fusion(f32[504,504]{1,0:T(8,128)S(1)} %fusion.17, bf16[256,2032]{1,0:T(8,128)(2,1)S(1)} %all_gather.6, bf16[256,504]{0,1:T(8,128)(2,1)S(1)} %copy-done.4), kind=kOutput, calls=%fused_computation.7 | convolution fusion | flops 131080320 | bytes 2060416 | tf_op jit(solution)/shard_map/dot_general | solution.py:11
  51.1 1.3 %fusion.15 = f32[504,504]{1,0:T(8,128)} fusion(bf16[256,2016]{0,1:T(8,128)(2,1)S(1)} %copy-done.6, s32[]{:T(128)S(6)} %select_n.130, bf16[256,248]{1,0:T(8,128)(2,1)S(1)} %multiply_convert_fusion.2, bf16[256,256]{1,0:T(8,128)(2,1)S(1)} %multiply_convert_fusion.3), kind=kOutput, calls=%fused_computation.41 | convolution fusion | flops 130572288 | bytes 1536260 | tf_op jit(solution)/shard_map/dot_general | solution.py:11
  52.3 8.4 %collective-permute-start.13 = (bf16[504,504]{1,0:T(8,128)(2,1)}, bf16[504,504]{1,0:T(8,128)(2,1)}, u32[]{:S(2)}, u32[]{:S(2)}) collective-permute-start(bf16[504,504]{1,0:T(8,128)(2,1)} %fusion.1), channel_id=1, source_target_pairs={{0,8},{8,0},{16,24},{24,16},{1,9},{9,1},{17,25},{25,17},{2,10},{10... | collective-permute-start | bytes 1524104 | tf_op jit(solution)/shard_map/ppermute | solution.py:50
  66.9 4.1 %all-to-all-start = ((bf16[4,64,1008]{2,1,0:T(8,128)(2,1)}), bf16[4,64,1008]{2,1,0:T(8,128)(2,1)}, u32[]{:S(2)}, u32[]{:S(2)}) async-start(bf16[4,64,1008]{2,1,0:T(8,128)(2,1)} %pad_maximum_fusion), calls=%async_computation | async-start | bytes 1048576 | tf_op jit(solution)/shard_map/all_to_all | solution.py:105
  71.0 1.2 %fusion = bf16[504,504]{1,0:T(8,128)(2,1)} fusion(f32[504,504]{1,0:T(8,128)S(1)} %fusion.13, bf16[256,504]{1,0:T(8,128)(2,1)S(1)} %constant_dynamic-update-slice_fusion.3, bf16[256,2032]{1,0:T(8,128)(2,1)S(1)} %all_gather.6), kind=kOutput, calls=%fused_computation.6 | convolution fusion | flops 130564224 | bytes 2064512 | tf_op jit(solution)/shard_map/dot_general | solution.py:11
  72.6 7.3 %all-to-all-done = bf16[4,64,1008]{2,1,0:T(8,128)(2,1)} async-done(((bf16[4,64,1008]{2,1,0:T(8,128)(2,1)}), bf16[4,64,1008]{2,1,0:T(8,128)(2,1)}, u32[]{:S(2)}, u32[]{:S(2)}) %all-to-all-start) | async-done | bytes 516128 | tf_op jit(solution)/shard_map/all_to_all | solution.py:105
  79.9 1.1 %slice_reduce_fusion.1 = (bf16[32,1008]{1,0:T(8,128)(2,1)S(1)}, bf16[32,1008]{1,0:T(8,128)(2,1)S(1)}) fusion(bf16[4,64,1008]{2,1,0:T(8,128)(2,1)} %all-to-all-done), kind=kLoop, calls=%fused_computation.33 | loop fusion | flops 193536 | bytes 645120 | tf_op jit(solution)/shard_map/reduce_sum | solution.py:107
  81.1 2.1 %convert_add_fusion = f32[504,504]{1,0:T(8,128)} fusion(f32[504,504]{1,0:T(8,128)S(1)} %convolution_add_fusion.1, bf16[504,504]{1,0:T(8,128)(2,1)} %collective-permute-done.13), kind=kLoop, calls=%fused_computation.12 | loop fusion | flops 508032 | bytes 2540160 | tf_op jit(solution)/shard_map/add | solution.py:122
  83.3 4.4 %collective-permute-done.10 = bf16[32,1008]{1,0:T(8,128)(2,1)S(1)} collective-permute-done((bf16[32,1008]{1,0:T(8,128)(2,1)S(1)}, bf16[32,1008]{1,0:T(8,128)(2,1)S(1)}, u32[]{:S(2)}, u32[]{:S(2)}) %collective-permute-start.10) | collective-permute-done | bytes 64544 | tf_op jit(solution)/shard_map/ppermute | solution.py:50
  87.9 10.2 %all_gather.7 = bf16[256,2016]{1,0:T(8,128)(2,1)S(1)} all-gather(bf16[32,2016]{1,0:T(8,128)(2,1)S(1)} %concatenate.31), channel_id=1, replica_groups=mesh['fs'=4,'tp'=8] {'tp'}, dimensions={0}, use_global_device_ids=true | all-gather | bytes 1161216 | tf_op jit(solution)/shard_map/all_gather | solution.py:53
  98.1 1.3 %copy.23 = bf16[256,2016]{0,1:T(8,128)(2,1)} copy(bf16[256,2016]{1,0:T(8,128)(2,1)S(1)} %all_gather.7) | data formatting | bytes 2064384
  99.4 2.1 %convert_add_fusion.1 = f32[504,504]{1,0:T(8,128)} fusion(f32[504,504]{1,0:T(8,128)S(1)} %convolution_add_fusion.3, bf16[504,504]{1,0:T(8,128)(2,1)} %collective-permute-done.11), kind=kLoop, calls=%fused_computation.13 | loop fusion | flops 508032 | bytes 2540160 | tf_op jit(solution)/shard_map/add | solution.py:127
  (77 shorter events, 16.0 us)
Async XLA Ops:
  0.6 29.4 %collective-permute-start.1 = (bf16[504,504]{1,0:T(8,128)(2,1)}, bf16[504,504]{1,0:T(8,128)(2,1)S(1)}, u32[]{:S(2)}, u32[]{:S(2)}) collective-permute-start(bf16[504,504]{1,0:T(8,128)(2,1)} %param.9), channel_id=1, source_target_pairs={{0,8},{8,0},{16,24},{24,16},{1,9},{9,1},{17,25},{25,17},{2,10},{10... | collective-permute-start | bytes 1524104 | tf_op jit(solution)/shard_map/ppermute | solution.py:50
  5.1 3.9 %copy-start.2 = (bf16[504,504]{1,0:T(8,128)(2,1)S(1)}, bf16[504,504]{1,0:T(8,128)(2,1)}, u32[]{:S(2)}) copy-start(bf16[504,504]{1,0:T(8,128)(2,1)} %param.8) | copy-start | bytes 1524100
  5.5 2.9 %copy-start.1 = (bf16[256,504]{0,1:T(8,128)(2,1)S(1)}, bf16[256,504]{0,1:T(8,128)(2,1)}, u32[]{:S(2)}) copy-start(bf16[256,504]{0,1:T(8,128)(2,1)} %param.6) | copy-start | bytes 774148
  5.7 13.2 %collective-permute-start = (bf16[32,2032]{1,0:T(8,128)(2,1)S(1)}, bf16[32,2032]{1,0:T(8,128)(2,1)S(1)}, u32[]{:S(2)}, u32[]{:S(2)}) collective-permute-start(bf16[32,2032]{1,0:T(8,128)(2,1)S(1)} %concatenate.24), channel_id=1, source_target_pairs={{0,16},{8,24},{16,0},{24,8},{1,17},{9,25},{17,1},{25,9},{2,18},{10... | collective-permute-start | bytes 390152 | tf_op jit(solution)/shard_map/ppermute | solution.py:50
  8.4 39.5 %collective-permute-start.12 = (bf16[256,504]{0,1:T(8,128)(2,1)S(1)}, bf16[256,504]{0,1:T(8,128)(2,1)S(1)}, u32[]{:S(2)}, u32[]{:S(2)}) collective-permute-start(bf16[256,504]{0,1:T(8,128)(2,1)S(1)} %copy-done.1), channel_id=1, source_target_pairs={{0,16},{8,24},{16,0},{24,8},{1,17},{9,25},{17,1},{25,9},{2,18},{10... | collective-permute-start | bytes 774152 | tf_op jit(solution)/shard_map/ppermute | solution.py:50
  9.7 51.4 %collective-permute-start.5 = (bf16[264,504]{1,0:T(8,128)(2,1)}, bf16[264,504]{1,0:T(8,128)(2,1)}, u32[]{:S(2)}, u32[]{:S(2)}) collective-permute-start(bf16[264,504]{1,0:T(8,128)(2,1)} %slice.68), channel_id=1, source_target_pairs={{0,8},{8,0},{16,24},{24,16},{1,9},{9,1},{17,25},{25,17},{2,10},{10... | collective-permute-start | bytes 798344 | tf_op jit(solution)/shard_map/ppermute | solution.py:50
  10.9 50.2 %collective-permute-start.4 = (bf16[240,504]{1,0:T(8,128)(2,1)}, bf16[240,504]{1,0:T(8,128)(2,1)}, u32[]{:S(2)}, u32[]{:S(2)}) collective-permute-start(bf16[240,504]{1,0:T(8,128)(2,1)} %slice.67), channel_id=1, source_target_pairs={{0,8},{8,0},{16,24},{24,16},{1,9},{9,1},{17,25},{25,17},{2,10},{10... | collective-permute-start | bytes 725768 | tf_op jit(solution)/shard_map/ppermute | solution.py:50
  12.8 17.2 %copy-start.7 = (bf16[504,504]{1,0:T(8,128)(2,1)S(1)}, bf16[504,504]{1,0:T(8,128)(2,1)}, u32[]{:S(2)}) copy-start(bf16[504,504]{1,0:T(8,128)(2,1)} %param.9) | copy-start | bytes 1524100
  30.0 4.5 %copy-start.8 = (bf16[504,504]{1,0:T(8,128)(2,1)}, bf16[504,504]{1,0:T(8,128)(2,1)S(1)}, u32[]{:S(2)}) copy-start(bf16[504,504]{1,0:T(8,128)(2,1)S(1)} %collective-permute-done.1) | copy-start | bytes 1524100
  31.0 4.5 %copy-start.5 = (bf16[256,2016]{0,1:T(8,128)(2,1)S(1)}, bf16[256,2016]{0,1:T(8,128)(2,1)}, u32[]{:S(2)}) copy-start(bf16[256,2016]{0,1:T(8,128)(2,1)} %param.7) | copy-start | bytes 3096580
  31.0 13.6 %collective-permute-start.3 = (bf16[256,248]{1,0:T(8,128)(2,1)}, bf16[256,248]{1,0:T(8,128)(2,1)S(1)}, u32[]{:S(2)}, u32[]{:S(2)}) collective-permute-start(bf16[256,248]{1,0:T(8,128)(2,1)} %convolution_convert_fusion.2), channel_id=1, source_target_pairs={{0,16},{8,24},{16,0},{24,8},{1,17},{9,25},{17,1},{25,9},{2,18},{10... | collective-permute-start | bytes 380936 | tf_op jit(solution)/shard_map/ppermute | solution.py:50
  35.5 1.0 %copy-start.9 = (bf16[504,504]{1,0:T(8,128)(2,1)S(1)}, bf16[504,504]{1,0:T(8,128)(2,1)}, u32[]{:S(2)}) copy-start(bf16[504,504]{1,0:T(8,128)(2,1)} %copy-done.8) | copy-start | bytes 1524100
  35.5 11.6 %collective-permute-start.2 = (bf16[256,256]{1,0:T(8,128)(2,1)}, bf16[256,256]{1,0:T(8,128)(2,1)S(1)}, u32[]{:S(2)}, u32[]{:S(2)}) collective-permute-start(bf16[256,256]{1,0:T(8,128)(2,1)} %convolution_convert_fusion.3), channel_id=1, source_target_pairs={{0,16},{8,24},{16,0},{24,8},{1,17},{9,25},{17,1},{25,9},{2,18},{10... | collective-permute-start | bytes 393224 | tf_op jit(solution)/shard_map/ppermute | solution.py:50
  39.9 7.3 %copy-start.10 = (f32[256,256]{1,0:T(8,128)S(1)}, f32[256,256]{1,0:T(8,128)}, u32[]{:S(2)}) copy-start(f32[256,256]{1,0:T(8,128)} %fusion.8) | copy-start | bytes 786436
  44.7 4.2 %copy-start.6 = (bf16[256,2016]{0,1:T(8,128)(2,1)S(1)}, bf16[256,2016]{0,1:T(8,128)(2,1)}, u32[]{:S(2)}) copy-start(bf16[256,2016]{0,1:T(8,128)(2,1)} %param.5) | copy-start | bytes 3096580
  44.7 19.0 %collective-permute-start.8 = (bf16[256,248]{1,0:T(8,128)(2,1)S(1)}, bf16[256,248]{1,0:T(8,128)(2,1)S(1)}, u32[]{:S(2)}, u32[]{:S(2)}) collective-permute-start(bf16[256,248]{1,0:T(8,128)(2,1)S(1)} %multiply_convert_fusion.2), channel_id=1, source_target_pairs={{0,16},{8,24},{16,0},{24,8},{1,17},{9,25},{17,1},{25,9},{2,18},{10... | collective-permute-start | bytes 380936 | tf_op jit(solution)/shard_map/ppermute | solution.py:50
  47.2 16.5 %collective-permute-start.7 = (bf16[256,256]{1,0:T(8,128)(2,1)S(1)}, bf16[256,256]{1,0:T(8,128)(2,1)S(1)}, u32[]{:S(2)}, u32[]{:S(2)}) collective-permute-start(bf16[256,256]{1,0:T(8,128)(2,1)S(1)} %multiply_convert_fusion.3), channel_id=1, source_target_pairs={{0,16},{8,24},{16,0},{24,8},{1,17},{9,25},{17,1},{25,9},{2,18},{10... | collective-permute-start | bytes 393224 | tf_op jit(solution)/shard_map/ppermute | solution.py:50
  52.3 28.8 %collective-permute-start.13 = (bf16[504,504]{1,0:T(8,128)(2,1)}, bf16[504,504]{1,0:T(8,128)(2,1)}, u32[]{:S(2)}, u32[]{:S(2)}) collective-permute-start(bf16[504,504]{1,0:T(8,128)(2,1)} %fusion.1), channel_id=1, source_target_pairs={{0,8},{8,0},{16,24},{24,16},{1,9},{9,1},{17,25},{25,17},{2,10},{10... | collective-permute-start | bytes 1524104 | tf_op jit(solution)/shard_map/ppermute | solution.py:50
  63.6 1.6 %collective-permute-start.6 = (bf16[4,32,1008]{2,1,0:T(8,128)(2,1)S(1)}, bf16[4,32,1008]{2,1,0:T(8,128)(2,1)S(1)}, u32[]{:S(2)}, u32[]{:S(2)}) collective-permute-start(bf16[4,32,1008]{2,1,0:T(8,128)(2,1)S(1)} %dynamic-slice_bitcast_fusion.1), channel_id=1, source_target_pairs={{0,1},{1,0},{2,3},{3,2},{4,5},{5,4},{6,7},{7,6},{8,9},{9,8},{10,11... | collective-permute-start | bytes 774152 | tf_op jit(solution)/shard_map/ppermute | solution.py:101
  64.2 1.7 %collective-permute-start.9 = (bf16[4,32,1008]{2,1,0:T(8,128)(2,1)S(1)}, bf16[4,32,1008]{2,1,0:T(8,128)(2,1)S(1)}, u32[]{:S(2)}, u32[]{:S(2)}) collective-permute-start(bf16[4,32,1008]{2,1,0:T(8,128)(2,1)S(1)} %dynamic-slice_bitcast_fusion), channel_id=1, source_target_pairs={{0,1},{1,0},{2,3},{3,2},{4,5},{5,4},{6,7},{7,6},{8,9},{9,8},{10,11... | collective-permute-start | bytes 774152 | tf_op jit(solution)/shard_map/ppermute | solution.py:101
  66.9 13.0 %all-to-all-start = ((bf16[4,64,1008]{2,1,0:T(8,128)(2,1)}), bf16[4,64,1008]{2,1,0:T(8,128)(2,1)}, u32[]{:S(2)}, u32[]{:S(2)}) async-start(bf16[4,64,1008]{2,1,0:T(8,128)(2,1)} %pad_maximum_fusion), calls=%async_computation | async-start | bytes 1048576 | tf_op jit(solution)/shard_map/all_to_all | solution.py:105
  71.0 1.3 %copy-start = (f32[504,504]{1,0:T(8,128)S(1)}, f32[504,504]{1,0:T(8,128)}, u32[]{:S(2)}) copy-start(f32[504,504]{1,0:T(8,128)} %fusion.15) | copy-start | bytes 3048196
  72.3 27.1 %collective-permute-start.11 = (bf16[504,504]{1,0:T(8,128)(2,1)}, bf16[504,504]{1,0:T(8,128)(2,1)}, u32[]{:S(2)}, u32[]{:S(2)}) collective-permute-start(bf16[504,504]{1,0:T(8,128)(2,1)} %fusion), channel_id=1, source_target_pairs={{0,8},{8,0},{16,24},{24,16},{1,9},{9,1},{17,25},{25,17},{2,10},{10... | collective-permute-start | bytes 1524104 | tf_op jit(solution)/shard_map/ppermute | solution.py:50
  81.0 6.7 %collective-permute-start.10 = (bf16[32,1008]{1,0:T(8,128)(2,1)S(1)}, bf16[32,1008]{1,0:T(8,128)(2,1)S(1)}, u32[]{:S(2)}, u32[]{:S(2)}) collective-permute-start(bf16[32,1008]{1,0:T(8,128)(2,1)S(1)} %get-tuple-element.22), channel_id=1, source_target_pairs={{0,16},{8,24},{16,0},{24,8},{1,17},{9,25},{17,1},{25,9},{2,18},{10... | collective-permute-start | bytes 193544 | tf_op jit(solution)/shard_map/ppermute | solution.py:50
  (2 other events, 1.6 us)

commit v5 on v4

--- a/solution.py
+++ b/solution.py
@@ -65,23 +65,26 @@
         route(jnp.concatenate([both(cotangent, row, share, k), gap, both(inputs, row, share, k)], axis=1), k, 0)
         for k in others
     ]
-    w_down_other = route(w_down, 0, 1)
-    gathered = [gather(s) for s in shares]
-    cot = [x[:, : 2 * block] for x in gathered]
-    w_down_g = jnp.concatenate([w_down, w_down_other], axis=1)
-    cut = block // 32 * 16
-    w_up_parts = [route(w_up[:cut], 0, 1), route(w_up[cut:], 0, 1)]
-    acts = [route(pre_act, k, 0) for k in others]
-
     units = pre_act.shape[1]
     half = (units // 2 + 15) // 16 * 16
     runs = [slice(0, half), slice(half, units)]
-    sent = [[dot(c, w_down_g[run], 1, 1).astype(BF16) for c in cot] for run in runs]
+    w_down_g = [route(w_down[run], 0, 1) for run in runs]
+    w_down_g = [jnp.concatenate([w_down[run], w], axis=1) for run, w in zip(runs, w_down_g)]
+    gathered = [gather(s) for s in shares]
+    cot = [x[:, : 2 * block] for x in gathered]
+    cut = block // 32 * 16
+    w_up_parts = [route(w_up[:cut], 0, 1)]
+    acts = [route(pre_act, k, 0) for k in others]
+
+    sent = []
+    for w in w_down_g:
+        sent.append([dot(c, w, 1, 1).astype(BF16) for c in cot])
     cotangent, inputs, w_up = lax.optimization_barrier((cotangent, inputs, w_up, sent))[:3]
+    w_up_parts.append(route(w_up[cut:], 0, 1))
     cot = [both(cotangent, 0, tokens, 0)] + cot
     pre_grad = []
     for n, run in enumerate(runs):
-        hidden_grad = lax.optimization_barrier(dot(cot[0], w_down_g[run], 1, 1))
+        hidden_grad = lax.optimization_barrier(dot(cot[0], w_down_g[n], 1, 1))
         for k in others:
             hidden_grad = hidden_grad + route(sent[n][k - 1], -k, 0).astype(F32)
         pre_grad.append((2.0 * positive(pre_act[:, run]) * hidden_grad).astype(BF16))

time: 102 us -> 95.2 us (0.933)
  starting transfers between devices: 25.9 us -> 19.9 us
  matrix products: 10.5 us -> 14.4 us
  local copies, waits for them, and re-layouts: 10.6 us -> 7 us
  waiting for transfers between devices: 25.7 us -> 22.7 us
  blocking collectives: 21.2 us -> 22.4 us
    ppermute x12 -> x13, starting transfers between devices: 21.1 us -> 15.1 us  [route(): return lax.ppermute(x, 'fs', pairs)]
    dot_general x14, matrix products: 10.5 us -> 14.4 us  [dot(): lax.dot_general(a, b, (((ca,), (cb,)), ((), ())), preferred_element_type=...]
    ppermute x12 -> x13, waiting for transfers between devices: 17.6 us -> 15 us  [route(): return lax.ppermute(x, 'fs', pairs)]
    unnamed x32 -> x36, local copies, waits for them, and re-layouts: 5.4 us -> 3.45 us
    all_gather x2, blocking collectives: 21.2 us -> 22.4 us  [gather(): return lax.all_gather(x, 'tp', axis=0, tiled=True)]
  transfers between devices with their start and end apart: 15 -> 16, of which waited for: 7 -> 8; matrix products, arithmetic and copies ran while one was open for 23% -> 25% of each run, Pallas kernels for 0% -> 0%
where the time goes in v5:
time: 95.2 us; the launch traced here: 94.1 us
  waiting for transfers between devices  22.7 us (24%)
  blocking collectives  22.4 us (24%)
  starting transfers between devices  19.9 us (21%)
  matrix products  14.4 us (15%)
  local copies, waits for them, and re-layouts  7 us (7%)
  other arithmetic  6.63 us (7%)
  between operations  1.17 us (1%)
    all_gather x2, blocking collectives, gather(): return lax.all_gather(x, 'tp', axis=0, tiled=True)  22.4 us
    ppermute x13, starting transfers between devices, route(): return lax.ppermute(x, 'fs', pairs)  15.1 us
    ppermute x13, waiting for transfers between devices, route(): return lax.ppermute(x, 'fs', pairs)  15 us
    dot_general x14, matrix products, dot(): lax.dot_general(a, b, (((ca,), (cb,)), ((), ())), preferred_element_type=...  14.4 us
    all_to_all x1, waiting for transfers between devices, body(): terms = lax.all_to_all(terms, 'tp', 0, 0, axis_index_groups=same_parity)  7.3 us
    all_to_all x1, starting transfers between devices, body(): terms = lax.all_to_all(terms, 'tp', 0, 0, axis_index_groups=same_parity)  4.16 us
    unnamed x36, local copies, waits for them, and re-layouts  3.45 us
    add x1, other arithmetic, body(): grad_down = kept + route(partial, 0, 1).astype(F32)  2.15 us
  transfers between devices with their start and end apart: 16, of which 8 were waited for; matrix products, arithmetic and copies ran while one was open for 25% of the time, Pallas kernels for 0%

profile of v5, /device:TPU:0, one launch (start us, length us, event | category | flops | bytes accessed | tf_op | source)
XLA Modules:
  0.0 94.1 jit_solution(14142311663654906919)
XLA Ops:
  0.7 1.3 %fusion.28 = (bf16[32,504]{0,1:T(8,128)(2,1)S(1)}, bf16[32,504]{0,1:T(8,128)(2,1)S(1)}, bf16[32,504]{0,1:T(8,128)(2,1)S(1)}, bf16[32,504]{0,1:T(8,128)(2,1)S(1)}) fusion(bf16[256,2016]{0,1:T(8,128)(2,1)} %param.5, s32[]{:T(128)S(6)} %select_n.125, s32[]{:T(128)S(6)} %select_n.128, s32[]{:T(128)S(6)} %select_n.127, bf16[256,2016]{0,1:T(8,128)(2,1)} %param.7), kind=kLoop, calls=%fused_computation.68 | loop fusion | bytes 258060 | tf_op jit(solution)/shard_map/dynamic_slice | solution.py:57
  2.7 4.1 %collective-permute-start = (bf16[32,2032]{1,0:T(8,128)(2,1)S(1)}, bf16[32,2032]{1,0:T(8,128)(2,1)S(1)}, u32[]{:S(2)}, u32[]{:S(2)}) collective-permute-start(bf16[32,2032]{1,0:T(8,128)(2,1)S(1)} %concatenate.27), channel_id=1, source_target_pairs={{0,16},{8,24},{16,0},{24,8},{1,17},{9,25},{17,1},{25,9},{2,18},{10... | collective-permute-start | bytes 390152 | tf_op jit(solution)/shard_map/ppermute | solution.py:50
  6.8 1.6 %collective-permute-start.2 = (bf16[248,504]{1,0:T(8,128)(2,1)S(1)}, bf16[248,504]{1,0:T(8,128)(2,1)}, u32[]{:S(2)}, u32[]{:S(2)}) collective-permute-start(bf16[248,504]{1,0:T(8,128)(2,1)S(1)} %slice.65), channel_id=1, source_target_pairs={{0,8},{8,0},{16,24},{24,16},{1,9},{9,1},{17,25},{25,17},{2,10},{10... | collective-permute-start | bytes 749960 | tf_op jit(solution)/shard_map/ppermute | solution.py:50
  10.1 1.6 %collective-permute-start.5 = (bf16[240,504]{1,0:T(8,128)(2,1)}, bf16[240,504]{1,0:T(8,128)(2,1)}, u32[]{:S(2)}, u32[]{:S(2)}) collective-permute-start(bf16[240,504]{1,0:T(8,128)(2,1)} %slice.67), channel_id=1, source_target_pairs={{0,8},{8,0},{16,24},{24,16},{1,9},{9,1},{17,25},{25,17},{2,10},{10... | collective-permute-start | bytes 725768 | tf_op jit(solution)/shard_map/ppermute | solution.py:50
  12.0 2.1 %collective-permute-done = bf16[32,2032]{1,0:T(8,128)(2,1)S(1)} collective-permute-done((bf16[32,2032]{1,0:T(8,128)(2,1)S(1)}, bf16[32,2032]{1,0:T(8,128)(2,1)S(1)}, u32[]{:S(2)}, u32[]{:S(2)}) %collective-permute-start) | collective-permute-done | bytes 130080 | tf_op jit(solution)/shard_map/ppermute | solution.py:50
  14.1 11.4 %all_gather.6 = bf16[256,2032]{1,0:T(8,128)(2,1)S(1)} all-gather(bf16[32,2032]{1,0:T(8,128)(2,1)S(1)} %collective-permute-done), channel_id=1, replica_groups=mesh['fs'=4,'tp'=8] {'tp'}, dimensions={0}, use_global_device_ids=true | all-gather | bytes 1170432 | tf_op jit(solution)/shard_map/all_gather | solution.py:53
  25.5 2.0 %convolution_convert_fusion.2 = bf16[256,248]{1,0:T(8,128)(2,1)} fusion(bf16[256,2032]{1,0:T(8,128)(2,1)S(1)} %all_gather.6, bf16[248,504]{1,0:T(8,128)(2,1)} %collective-permute-done.2, bf16[248,504]{1,0:T(8,128)(2,1)S(1)} %slice.65), kind=kOutput, calls=%fused_computation.8 | convolution fusion | flops 129055232 | bytes 1155200 | tf_op jit(solution)/shard_map/dot_general | solution.py:11
  28.8 2.0 %convolution_convert_fusion.3 = bf16[256,256]{1,0:T(8,128)(2,1)} fusion(bf16[256,2032]{1,0:T(8,128)(2,1)S(1)} %all_gather.6, bf16[256,504]{1,0:T(8,128)(2,1)} %collective-permute-done.1, bf16[256,504]{1,0:T(8,128)(2,1)S(1)} %slice.64), kind=kOutput, calls=%fused_computation.9 | convolution fusion | flops 133218304 | bytes 1175552 | tf_op jit(solution)/shard_map/dot_general | solution.py:11
  30.8 1.7 %collective-permute-start.3 = (bf16[256,256]{1,0:T(8,128)(2,1)}, bf16[256,256]{1,0:T(8,128)(2,1)S(1)}, u32[]{:S(2)}, u32[]{:S(2)}) collective-permute-start(bf16[256,256]{1,0:T(8,128)(2,1)} %convolution_convert_fusion.3), channel_id=1, source_target_pairs={{0,16},{8,24},{16,0},{24,8},{1,17},{9,25},{17,1},{25,9},{2,18},{10... | collective-permute-start | bytes 393224 | tf_op jit(solution)/shard_map/ppermute | solution.py:50
  32.5 2.2 %fusion.6 = f32[256,256]{1,0:T(8,128)} fusion(bf16[256,504]{1,0:T(8,128)(2,1)} %collective-permute-done.1, bf16[256,504]{1,0:T(8,128)(2,1)S(1)} %copy-done.9, bf16[256,504]{0,1:T(8,128)(2,1)S(1)} %get-tuple-element.25, bf16[256,504]{0,1:T(8,128)(2,1)S(1)} %get-tuple-element.24), kind=kOutput, calls=%fused_computation.24 | convolution fusion | flops 134184960 | bytes 1294336 | tf_op jit(solution)/shard_map/dot_general | solution.py:11
  34.7 2.0 %fusion.7 = f32[256,248]{0,1:T(8,128)} fusion(bf16[256,504]{0,1:T(8,128)(2,1)S(1)} %get-tuple-element.25, bf16[256,504]{0,1:T(8,128)(2,1)S(1)} %get-tuple-element.24, bf16[248,504]{1,0:T(8,128)(2,1)} %collective-permute-done.2, bf16[248,504]{1,0:T(8,128)(2,1)S(1)} %copy-done.12), kind=kOutput, calls=%fused_computation.25 | convolution fusion | flops 130023936 | bytes 1270016 | tf_op jit(solution)/shard_map/dot_general | solution.py:11
  37.8 1.5 %collective-permute-start.6 = (bf16[264,504]{1,0:T(8,128)(2,1)S(1)}, bf16[264,504]{1,0:T(8,128)(2,1)S(1)}, u32[]{:S(2)}, u32[]{:S(2)}) collective-permute-start(bf16[264,504]{1,0:T(8,128)(2,1)S(1)} %slice.68), channel_id=1, source_target_pairs={{0,8},{8,0},{16,24},{24,16},{1,9},{9,1},{17,25},{25,17},{2,10},{10... | collective-permute-start | bytes 798344 | tf_op jit(solution)/shard_map/ppermute | solution.py:50
  39.3 1.4 %collective-permute-done.4 = bf16[256,248]{1,0:T(8,128)(2,1)S(1)} collective-permute-done((bf16[256,248]{1,0:T(8,128)(2,1)}, bf16[256,248]{1,0:T(8,128)(2,1)S(1)}, u32[]{:S(2)}, u32[]{:S(2)}) %collective-permute-start.4) | collective-permute-done | bytes 127008 | tf_op jit(solution)/shard_map/ppermute | solution.py:50
  41.1 1.8 %collective-permute-done.3 = bf16[256,256]{1,0:T(8,128)(2,1)S(1)} collective-permute-done((bf16[256,256]{1,0:T(8,128)(2,1)}, bf16[256,256]{1,0:T(8,128)(2,1)S(1)}, u32[]{:S(2)}, u32[]{:S(2)}) %collective-permute-start.3) | collective-permute-done | bytes 131104 | tf_op jit(solution)/shard_map/ppermute | solution.py:50
  46.1 1.3 %fusion.14 = f32[504,504]{1,0:T(8,128)} fusion(bf16[256,2016]{0,1:T(8,128)(2,1)S(1)} %copy-done.6, s32[]{:T(128)S(6)} %select_n.130, bf16[256,248]{1,0:T(8,128)(2,1)S(1)} %multiply_convert_fusion.2, bf16[256,256]{1,0:T(8,128)(2,1)S(1)} %multiply_convert_fusion.3), kind=kOutput, calls=%fused_computation.39 | convolution fusion | flops 130572288 | bytes 1536260 | tf_op jit(solution)/shard_map/dot_general | solution.py:11
  47.3 2.2 %collective-permute-start.14 = (bf16[504,504]{1,0:T(8,128)(2,1)}, bf16[504,504]{1,0:T(8,128)(2,1)}, u32[]{:S(2)}, u32[]{:S(2)}) collective-permute-start(bf16[504,504]{1,0:T(8,128)(2,1)} %fusion.1), channel_id=1, source_target_pairs={{0,8},{8,0},{16,24},{24,16},{1,9},{9,1},{17,25},{25,17},{2,10},{10... | collective-permute-start | bytes 1524104 | tf_op jit(solution)/shard_map/ppermute | solution.py:50
  49.6 5.6 %collective-permute-done.8 = bf16[256,256]{1,0:T(8,128)(2,1)S(1)} collective-permute-done((bf16[256,256]{1,0:T(8,128)(2,1)S(1)}, bf16[256,256]{1,0:T(8,128)(2,1)S(1)}, u32[]{:S(2)}, u32[]{:S(2)}) %collective-permute-start.8) | collective-permute-done | bytes 131104 | tf_op jit(solution)/shard_map/ppermute | solution.py:50
  60.0 4.2 %all-to-all-start = ((bf16[4,64,1008]{2,1,0:T(8,128)(2,1)}), bf16[4,64,1008]{2,1,0:T(8,128)(2,1)}, u32[]{:S(2)}, u32[]{:S(2)}) async-start(bf16[4,64,1008]{2,1,0:T(8,128)(2,1)} %pad_maximum_fusion.1), calls=%async_computation | async-start | bytes 1048576 | tf_op jit(solution)/shard_map/all_to_all | solution.py:108
  65.7 7.3 %all-to-all-done = bf16[4,64,1008]{2,1,0:T(8,128)(2,1)} async-done(((bf16[4,64,1008]{2,1,0:T(8,128)(2,1)}), bf16[4,64,1008]{2,1,0:T(8,128)(2,1)}, u32[]{:S(2)}, u32[]{:S(2)}) %all-to-all-start) | async-done | bytes 516128 | tf_op jit(solution)/shard_map/all_to_all | solution.py:108
  74.3 2.1 %convert_add_fusion = f32[504,504]{1,0:T(8,128)} fusion(f32[504,504]{1,0:T(8,128)S(1)} %convolution_add_fusion.1, bf16[504,504]{1,0:T(8,128)(2,1)} %collective-permute-done.14), kind=kLoop, calls=%fused_computation.10 | loop fusion | flops 508032 | bytes 2540160 | tf_op jit(solution)/shard_map/add | solution.py:125
  76.4 3.1 %collective-permute-done.11 = bf16[32,1008]{1,0:T(8,128)(2,1)S(1)} collective-permute-done((bf16[32,1008]{1,0:T(8,128)(2,1)S(1)}, bf16[32,1008]{1,0:T(8,128)(2,1)S(1)}, u32[]{:S(2)}, u32[]{:S(2)}) %collective-permute-start.11) | collective-permute-done | bytes 64544 | tf_op jit(solution)/shard_map/ppermute | solution.py:50
  79.7 10.9 %all_gather.7 = bf16[256,2016]{1,0:T(8,128)(2,1)S(1)} all-gather(bf16[32,2016]{1,0:T(8,128)(2,1)S(1)} %concatenate.35), channel_id=1, replica_groups=mesh['fs'=4,'tp'=8] {'tp'}, dimensions={0}, use_global_device_ids=true | all-gather | bytes 1161216 | tf_op jit(solution)/shard_map/all_gather | solution.py:53
  90.6 1.3 %copy.23 = bf16[256,2016]{0,1:T(8,128)(2,1)} copy(bf16[256,2016]{1,0:T(8,128)(2,1)S(1)} %all_gather.7) | data formatting | bytes 2064384
  92.0 2.1 %convert_add_fusion.1 = f32[504,504]{1,0:T(8,128)} fusion(f32[504,504]{1,0:T(8,128)S(1)} %convolution_add_fusion.3, bf16[504,504]{1,0:T(8,128)(2,1)} %collective-permute-done.12), kind=kLoop, calls=%fused_computation.11 | loop fusion | flops 508032 | bytes 2540160 | tf_op jit(solution)/shard_map/add | solution.py:130
  (85 shorter events, 16.1 us)
Async XLA Ops:
  2.0 4.8 %copy-start.7 = (bf16[504,504]{1,0:T(8,128)(2,1)S(1)}, bf16[504,504]{1,0:T(8,128)(2,1)}, u32[]{:S(2)}) copy-start(bf16[504,504]{1,0:T(8,128)(2,1)} %param.9) | copy-start | bytes 1524100
  2.7 6.7 %copy-start.2 = (bf16[504,504]{1,0:T(8,128)(2,1)S(1)}, bf16[504,504]{1,0:T(8,128)(2,1)}, u32[]{:S(2)}) copy-start(bf16[504,504]{1,0:T(8,128)(2,1)} %param.8) | copy-start | bytes 1524100
  2.7 11.4 %collective-permute-start = (bf16[32,2032]{1,0:T(8,128)(2,1)S(1)}, bf16[32,2032]{1,0:T(8,128)(2,1)S(1)}, u32[]{:S(2)}, u32[]{:S(2)}) collective-permute-start(bf16[32,2032]{1,0:T(8,128)(2,1)S(1)} %concatenate.27), channel_id=1, source_target_pairs={{0,16},{8,24},{16,0},{24,8},{1,17},{9,25},{17,1},{25,9},{2,18},{10... | collective-permute-start | bytes 390152 | tf_op jit(solution)/shard_map/ppermute | solution.py:50
  6.8 18.7 %copy-start.11 = (bf16[248,504]{1,0:T(8,128)(2,1)}, bf16[248,504]{1,0:T(8,128)(2,1)S(1)}, u32[]{:S(2)}) copy-start(bf16[248,504]{1,0:T(8,128)(2,1)S(1)} %slice.65) | copy-start | bytes 749956
  6.8 2.2 %copy-start.1 = (bf16[256,504]{0,1:T(8,128)(2,1)S(1)}, bf16[256,504]{0,1:T(8,128)(2,1)}, u32[]{:S(2)}) copy-start(bf16[256,504]{0,1:T(8,128)(2,1)} %param.6) | copy-start | bytes 774148
  6.8 18.7 %collective-permute-start.2 = (bf16[248,504]{1,0:T(8,128)(2,1)S(1)}, bf16[248,504]{1,0:T(8,128)(2,1)}, u32[]{:S(2)}, u32[]{:S(2)}) collective-permute-start(bf16[248,504]{1,0:T(8,128)(2,1)S(1)} %slice.65), channel_id=1, source_target_pairs={{0,8},{8,0},{16,24},{24,16},{1,9},{9,1},{17,25},{25,17},{2,10},{10... | collective-permute-start | bytes 749960 | tf_op jit(solution)/shard_map/ppermute | solution.py:50
  8.5 20.3 %copy-start.8 = (bf16[256,504]{1,0:T(8,128)(2,1)}, bf16[256,504]{1,0:T(8,128)(2,1)S(1)}, u32[]{:S(2)}) copy-start(bf16[256,504]{1,0:T(8,128)(2,1)S(1)} %slice.64) | copy-start | bytes 774148
  8.5 20.3 %collective-permute-start.1 = (bf16[256,504]{1,0:T(8,128)(2,1)S(1)}, bf16[256,504]{1,0:T(8,128)(2,1)}, u32[]{:S(2)}, u32[]{:S(2)}) collective-permute-start(bf16[256,504]{1,0:T(8,128)(2,1)S(1)} %slice.64), channel_id=1, source_target_pairs={{0,8},{8,0},{16,24},{24,16},{1,9},{9,1},{17,25},{25,17},{2,10},{10... | collective-permute-start | bytes 774152 | tf_op jit(solution)/shard_map/ppermute | solution.py:50
  9.0 33.9 %collective-permute-start.13 = (bf16[256,504]{0,1:T(8,128)(2,1)S(1)}, bf16[256,504]{0,1:T(8,128)(2,1)S(1)}, u32[]{:S(2)}, u32[]{:S(2)}) collective-permute-start(bf16[256,504]{0,1:T(8,128)(2,1)S(1)} %copy-done.1), channel_id=1, source_target_pairs={{0,16},{8,24},{16,0},{24,8},{1,17},{9,25},{17,1},{25,9},{2,18},{10... | collective-permute-start | bytes 774152 | tf_op jit(solution)/shard_map/ppermute | solution.py:50
  10.1 45.1 %collective-permute-start.5 = (bf16[240,504]{1,0:T(8,128)(2,1)}, bf16[240,504]{1,0:T(8,128)(2,1)}, u32[]{:S(2)}, u32[]{:S(2)}) collective-permute-start(bf16[240,504]{1,0:T(8,128)(2,1)} %slice.67), channel_id=1, source_target_pairs={{0,8},{8,0},{16,24},{24,16},{1,9},{9,1},{17,25},{25,17},{2,10},{10... | collective-permute-start | bytes 725768 | tf_op jit(solution)/shard_map/ppermute | solution.py:50
  27.5 4.9 %copy-start.5 = (bf16[256,2016]{0,1:T(8,128)(2,1)S(1)}, bf16[256,2016]{0,1:T(8,128)(2,1)}, u32[]{:S(2)}) copy-start(bf16[256,2016]{0,1:T(8,128)(2,1)} %param.7) | copy-start | bytes 3096580
  27.5 13.1 %collective-permute-start.4 = (bf16[256,248]{1,0:T(8,128)(2,1)}, bf16[256,248]{1,0:T(8,128)(2,1)S(1)}, u32[]{:S(2)}, u32[]{:S(2)}) collective-permute-start(bf16[256,248]{1,0:T(8,128)(2,1)} %convolution_convert_fusion.2), channel_id=1, source_target_pairs={{0,16},{8,24},{16,0},{24,8},{1,17},{9,25},{17,1},{25,9},{2,18},{10... | collective-permute-start | bytes 380936 | tf_op jit(solution)/shard_map/ppermute | solution.py:50
  30.8 12.1 %collective-permute-start.3 = (bf16[256,256]{1,0:T(8,128)(2,1)}, bf16[256,256]{1,0:T(8,128)(2,1)S(1)}, u32[]{:S(2)}, u32[]{:S(2)}) collective-permute-start(bf16[256,256]{1,0:T(8,128)(2,1)} %convolution_convert_fusion.3), channel_id=1, source_target_pairs={{0,16},{8,24},{16,0},{24,8},{1,17},{9,25},{17,1},{25,9},{2,18},{10... | collective-permute-start | bytes 393224 | tf_op jit(solution)/shard_map/ppermute | solution.py:50
  32.5 2.2 %copy-start.12 = (bf16[248,504]{1,0:T(8,128)(2,1)S(1)}, bf16[248,504]{1,0:T(8,128)(2,1)}, u32[]{:S(2)}) copy-start(bf16[248,504]{1,0:T(8,128)(2,1)} %copy-done.11) | copy-start | bytes 749956
  37.8 17.5 %collective-permute-start.6 = (bf16[264,504]{1,0:T(8,128)(2,1)S(1)}, bf16[264,504]{1,0:T(8,128)(2,1)S(1)}, u32[]{:S(2)}, u32[]{:S(2)}) collective-permute-start(bf16[264,504]{1,0:T(8,128)(2,1)S(1)} %slice.68), channel_id=1, source_target_pairs={{0,8},{8,0},{16,24},{24,16},{1,9},{9,1},{17,25},{25,17},{2,10},{10... | collective-permute-start | bytes 798344 | tf_op jit(solution)/shard_map/ppermute | solution.py:50
  39.3 3.6 %copy-start.10 = (f32[256,256]{1,0:T(8,128)S(1)}, f32[256,256]{1,0:T(8,128)}, u32[]{:S(2)}) copy-start(f32[256,256]{1,0:T(8,128)} %fusion.6) | copy-start | bytes 786436
  40.7 14.5 %collective-permute-start.9 = (bf16[256,248]{1,0:T(8,128)(2,1)S(1)}, bf16[256,248]{1,0:T(8,128)(2,1)S(1)}, u32[]{:S(2)}, u32[]{:S(2)}) collective-permute-start(bf16[256,248]{1,0:T(8,128)(2,1)S(1)} %multiply_convert_fusion.2), channel_id=1, source_target_pairs={{0,16},{8,24},{16,0},{24,8},{1,17},{9,25},{17,1},{25,9},{2,18},{10... | collective-permute-start | bytes 380936 | tf_op jit(solution)/shard_map/ppermute | solution.py:50
  43.7 11.5 %collective-permute-start.8 = (bf16[256,256]{1,0:T(8,128)(2,1)S(1)}, bf16[256,256]{1,0:T(8,128)(2,1)S(1)}, u32[]{:S(2)}, u32[]{:S(2)}) collective-permute-start(bf16[256,256]{1,0:T(8,128)(2,1)S(1)} %multiply_convert_fusion.3), channel_id=1, source_target_pairs={{0,16},{8,24},{16,0},{24,8},{1,17},{9,25},{17,1},{25,9},{2,18},{10... | collective-permute-start | bytes 393224 | tf_op jit(solution)/shard_map/ppermute | solution.py:50
  47.3 26.9 %collective-permute-start.14 = (bf16[504,504]{1,0:T(8,128)(2,1)}, bf16[504,504]{1,0:T(8,128)(2,1)}, u32[]{:S(2)}, u32[]{:S(2)}) collective-permute-start(bf16[504,504]{1,0:T(8,128)(2,1)} %fusion.1), channel_id=1, source_target_pairs={{0,8},{8,0},{16,24},{24,16},{1,9},{9,1},{17,25},{25,17},{2,10},{10... | collective-permute-start | bytes 1524104 | tf_op jit(solution)/shard_map/ppermute | solution.py:50
  56.7 1.8 %collective-permute-start.7 = (bf16[4,32,1008]{2,1,0:T(8,128)(2,1)S(1)}, bf16[4,32,1008]{2,1,0:T(8,128)(2,1)S(1)}, u32[]{:S(2)}, u32[]{:S(2)}) collective-permute-start(bf16[4,32,1008]{2,1,0:T(8,128)(2,1)S(1)} %dynamic-slice_bitcast_fusion.1), channel_id=1, source_target_pairs={{0,1},{1,0},{2,3},{3,2},{4,5},{5,4},{6,7},{7,6},{8,9},{9,8},{10,11... | collective-permute-start | bytes 774152 | tf_op jit(solution)/shard_map/ppermute | solution.py:104
  57.4 1.7 %collective-permute-start.10 = (bf16[4,32,1008]{2,1,0:T(8,128)(2,1)S(1)}, bf16[4,32,1008]{2,1,0:T(8,128)(2,1)S(1)}, u32[]{:S(2)}, u32[]{:S(2)}) collective-permute-start(bf16[4,32,1008]{2,1,0:T(8,128)(2,1)S(1)} %dynamic-slice_bitcast_fusion), channel_id=1, source_target_pairs={{0,1},{1,0},{2,3},{3,2},{4,5},{5,4},{6,7},{7,6},{8,9},{9,8},{10,11... | collective-permute-start | bytes 774152 | tf_op jit(solution)/shard_map/ppermute | solution.py:104
  60.0 13.1 %all-to-all-start = ((bf16[4,64,1008]{2,1,0:T(8,128)(2,1)}), bf16[4,64,1008]{2,1,0:T(8,128)(2,1)}, u32[]{:S(2)}, u32[]{:S(2)}) async-start(bf16[4,64,1008]{2,1,0:T(8,128)(2,1)} %pad_maximum_fusion.1), calls=%async_computation | async-start | bytes 1048576 | tf_op jit(solution)/shard_map/all_to_all | solution.py:108
  65.4 26.5 %collective-permute-start.12 = (bf16[504,504]{1,0:T(8,128)(2,1)}, bf16[504,504]{1,0:T(8,128)(2,1)}, u32[]{:S(2)}, u32[]{:S(2)}) collective-permute-start(bf16[504,504]{1,0:T(8,128)(2,1)} %fusion), channel_id=1, source_target_pairs={{0,8},{8,0},{16,24},{24,16},{1,9},{9,1},{17,25},{25,17},{2,10},{10... | collective-permute-start | bytes 1524104 | tf_op jit(solution)/shard_map/ppermute | solution.py:50
  74.2 5.3 %collective-permute-start.11 = (bf16[32,1008]{1,0:T(8,128)(2,1)S(1)}, bf16[32,1008]{1,0:T(8,128)(2,1)S(1)}, u32[]{:S(2)}, u32[]{:S(2)}) collective-permute-start(bf16[32,1008]{1,0:T(8,128)(2,1)S(1)} %get-tuple-element.22), channel_id=1, source_target_pairs={{0,16},{8,24},{16,0},{24,8},{1,17},{9,25},{17,1},{25,9},{2,18},{10... | collective-permute-start | bytes 193544 | tf_op jit(solution)/shard_map/ppermute | solution.py:50
  (5 other events, 7.0 us)
